TPU v7x, 32 devices: a whole 2x2x4 slice. The times are simulated.
32 devices in a mesh: sp: 8 (over z, x), tp: 4 (over y, core).
Axes of the slice: x: 2, y: 2, z: 4, core: 2. Of those that a mesh axis runs over, the one named last changes fastest.
Arguments:
- mixer_input: bfloat16 [2048, 1024], P('sp', 'tp'), may hold values from -8 to 8
- decay_shift: float32 [2048, 64], P('sp', 'tp'), may hold values from -2.3 to 0
- pole_real: float32 [64, 64], P('tp'), may hold values from -1 to 0
- pole_imaginary: float32 [64, 64], P('tp'), may hold values from 1 to 201.06176
- log_step: float32 [64], P('tp'), may hold values from -4.15 to -3
- input_map: float32 [2, 64, 64, 16], P(None, 'tp'), may hold values from -1 to 1
- readout_matrix: float32 [2, 64, 16, 64], P(None, 'tp'), may hold values from -0.5 to 0.5
- skip: float32 [1024], P('tp'), may hold values from -6 to 6
- out_proj: bfloat16 [1024, 2048], P('tp'), may hold values from -0.1875 to 0.1875
- stream: bfloat16 [2048, 2048], P(('sp', 'tp')), may hold values from -6 to 6
- norm_gain: float32 [2048], replicated, may hold values from 0.1 to 1.9
- routes: int32 [2048, 2], P(('sp', 'tp')), may hold values from 0 to 7, all different within a row; in each aligned block of 64 rows (0 to 63, 64 to 127, ...) at most 32 rows name the same one
- route_logits: float32 [2048, 2], P(('sp', 'tp')), may hold values from -7.5 to 7.5
- w_gate: bfloat16 [8, 2048, 7168], P('sp', None, 'tp'), may hold values from -0.125 to 0.125
- w_up: bfloat16 [8, 2048, 7168], P('sp', None, 'tp'), may hold values from -0.125 to 0.125
- w_down: bfloat16 [8, 7168, 2048], P('sp', 'tp'), may hold values from -0.21875 to 0.21875
Outputs:
- layer_out: bfloat16 [2048, 2048], P(('sp', 'tp'))
Inputs may be any that keep to these rules, and one draw needn't show every extreme that they name: `routes`: in the rows of one device no expert is named more than 32 times, a bound that some block reaches; the 2 experts of a token differ.
All inputs are finite; a program needn't handle non-finite values.
Results may differ from a plain program's by a relative error of at most 0.015.
Values may be sent and summed in bfloat16 or wider, within the bound.
A program may use at most 128 MiB of HBM per device.

v0:
```python
import functools

import jax
import jax.numpy as jnp
from jax import lax
from jax.experimental import pallas as pl
from jax.experimental.pallas import tpu as pltpu
from jax.sharding import PartitionSpec as P

TOP_PRECISION = lax.Precision.HIGHEST
EPS = 1e-06
LANES = 8
MESH = pl.DeviceIdType.MESH


def discretize(pole_real, pole_imaginary, log_step, input_map):
    step = jnp.exp(log_step)[:, None]
    magnitude = jnp.exp(pole_real * step)
    factor_real = magnitude * jnp.cos(pole_imaginary * step)
    factor_imaginary = magnitude * jnp.sin(pole_imaginary * step)
    denominator = pole_real * pole_real + pole_imaginary * pole_imaginary
    ratio_real = ((factor_real - 1.0) * pole_real + factor_imaginary * pole_imaginary) / denominator
    ratio_imaginary = (
        factor_imaginary * pole_real - (factor_real - 1.0) * pole_imaginary
    ) / denominator
    map_real = ratio_real[:, :, None] * input_map[0] - ratio_imaginary[:, :, None] * input_map[1]
    map_imaginary = (
        ratio_real[:, :, None] * input_map[1] + ratio_imaginary[:, :, None] * input_map[0]
    )
    return (factor_real, factor_imaginary, map_real, map_imaginary)


def on_ring(body, axis):
    count, mine = lax.axis_size(axis), lax.axis_index(axis)
    barrier = pltpu.get_barrier_semaphore()
    for ahead in range(1, count):
        pl.semaphore_signal(
            barrier,
            inc=1,
            device_id={axis: lax.rem(mine + ahead, count)},
            device_id_type=MESH,
        )
    pl.semaphore_wait(barrier, count - 1)
    body(count, mine)


def exchange_kernel(axis, gather, value, result, send, receive, own):
    def body(count, mine):
        copies = []
        for ahead in range(1, count):
            peer = lax.rem(mine + ahead, count)
            copy = pltpu.make_async_remote_copy(
                src_ref=value if gather else value.at[peer],
                dst_ref=result.at[mine],
                send_sem=send.at[ahead],
                recv_sem=receive.at[ahead],
                device_id={axis: peer},
                device_id_type=MESH,
            )
            copy.start()
            copies.append(copy)
        kept = pltpu.make_async_copy(value if gather else value.at[mine], result.at[mine], own)
        kept.start()
        kept.wait()
        for copy in copies:
            copy.wait()

    on_ring(body, axis)


def exchange(value, axis, number, gather=False):
    count = lax.axis_size(axis)
    shape = ((count,) + value.shape) if gather else value.shape
    return pl.pallas_call(
        functools.partial(exchange_kernel, axis, gather),
        out_shape=jax.ShapeDtypeStruct(shape, value.dtype),
        in_specs=[pl.BlockSpec(memory_space=pltpu.VMEM)],
        out_specs=pl.BlockSpec(memory_space=pltpu.VMEM),
        scratch_shapes=[
            pltpu.SemaphoreType.DMA((count,)),
            pltpu.SemaphoreType.DMA((count,)),
            pltpu.SemaphoreType.DMA,
        ],
        compiler_params=pltpu.CompilerParams(collective_id=number, has_side_effects=True),
        name=f"exchange_{number}",
    )(value)


def across(left, right):
    return lax.dot_general(
        left, right, (((1,), (1,)), ((), ())), preferred_element_type=jnp.float32
    )


def prepare(values, shift, maps, scale, drive_real, drive_imaginary):
    groups, width = shift.shape[1], scale.shape[1]
    spread = lax.broadcasted_iota(jnp.int32, (groups, width), 1) // (width // groups)
    hot = (spread == lax.broadcasted_iota(jnp.int32, (groups, width), 0)).astype(jnp.float32)
    scale[...] = jnp.dot(
        jnp.exp(shift[...]), hot, precision=TOP_PRECISION, preferred_element_type=jnp.float32
    )
    entries = values[...]
    drive_real[...] = across(entries, maps[0]) + across(entries, maps[1])
    drive_imaginary[...] = across(entries, maps[2]) + across(entries, maps[3])


def totals_kernel(values, shift, factor, maps, parts, total, scale, drive_real, drive_imaginary):
    prepare(values, shift, maps, scale, drive_real, drive_imaginary)
    width = scale.shape[1]
    wide = (LANES, width)
    factor_real = jnp.broadcast_to(factor[0:1, :], wide)
    factor_imaginary = jnp.broadcast_to(factor[1:2, :], wide)

    def step(position, carry):
        a_real, a_imaginary, x_real, x_imaginary = carry
        rows = pl.ds(pl.multiple_of(position * LANES, LANES), LANES)
        grow = scale[rows, :]
        b_real, b_imaginary = grow * factor_real, grow * factor_imaginary
        return (
            b_real * a_real - b_imaginary * a_imaginary,
            b_real * a_imaginary + b_imaginary * a_real,
            b_real * x_real - b_imaginary * x_imaginary + drive_real[rows, :],
            b_real * x_imaginary + b_imaginary * x_real + drive_imaginary[rows, :],
        )

    empty = jnp.zeros(wide, jnp.float32)
    ends = lax.fori_loop(
        0, scale.shape[0] // LANES, step, (jnp.ones(wide, jnp.float32), empty, empty, empty)
    )
    for place, end in enumerate(ends):
        parts[place] = end
    run = tuple(end[0:1] for end in ends)
    for segment in range(1, LANES):
        b_real, b_imaginary, y_real, y_imaginary = (
            end[segment : segment + 1] for end in ends
        )
        a_real, a_imaginary, x_real, x_imaginary = run
        run = (
            b_real * a_real - b_imaginary * a_imaginary,
            b_real * a_imaginary + b_imaginary * a_real,
            b_real * x_real - b_imaginary * x_imaginary + y_real,
            b_real * x_imaginary + b_imaginary * x_real + y_imaginary,
        )
    total[...] = jnp.concatenate(run + (jnp.zeros((LANES - 4, width), jnp.float32),), axis=0)


def split(value):
    high = value.astype(jnp.bfloat16)
    return high, (value - high.astype(jnp.float32)).astype(jnp.bfloat16)


def respond_kernel(
    axis, values, shift, factor, maps, parts, gathered, reads, skip, out,
    scale, drive_real, drive_imaginary,
):
    prepare(values, shift, maps, scale, drive_real, drive_imaginary)
    width = scale.shape[1]
    mine = lax.axis_index(axis)

    def before(position, carry):
        real, imaginary = carry
        item = gathered[position]
        a_real, a_imaginary = item[0:1], item[1:2]
        keep = position < mine
        return (
            jnp.where(keep, a_real * real - a_imaginary * imaginary + item[2:3], real),
            jnp.where(keep, a_real * imaginary + a_imaginary * real + item[3:4], imaginary),
        )

    none = jnp.zeros((1, width), jnp.float32)
    real, imaginary = lax.fori_loop(0, gathered.shape[0] - 1, before, (none, none))
    reals, imaginaries = [real], [imaginary]
    for segment in range(LANES - 1):
        at = slice(segment, segment + 1)
        a_real, a_imaginary = parts[0, at, :], parts[1, at, :]
        real, imaginary = (
            a_real * real - a_imaginary * imaginary + parts[2, at, :],
            a_real * imaginary + a_imaginary * real + parts[3, at, :],
        )
        reals.append(real)
        imaginaries.append(imaginary)
    wide = (LANES, width)
    factor_real = jnp.broadcast_to(factor[0:1, :], wide)
    factor_imaginary = jnp.broadcast_to(factor[1:2, :], wide)

    def step(position, carry):
        x_real, x_imaginary = carry
        rows = pl.ds(pl.multiple_of(position * LANES, LANES), LANES)
        grow = scale[rows, :]
        b_real, b_imaginary = grow * factor_real, grow * factor_imaginary
        new_real = b_real * x_real - b_imaginary * x_imaginary + drive_real[rows, :]
        new_imaginary = b_real * x_imaginary + b_imaginary * x_real + drive_imaginary[rows, :]
        drive_real[rows, :] = new_real
        drive_imaginary[rows, :] = new_imaginary
        return new_real, new_imaginary

    lax.fori_loop(
        0,
        scale.shape[0] // LANES,
        step,
        (jnp.concatenate(reals, axis=0), jnp.concatenate(imaginaries, axis=0)),
    )
    high, low = split(drive_real[...])
    response = across(high, reads[0]) + across(low, reads[0]) + across(high, reads[1])
    high, low = split(drive_imaginary[...])
    response -= across(high, reads[2]) + across(low, reads[2]) + across(high, reads[3])
    response += skip[...] * values[...].astype(jnp.float32)
    out[...] = jax.nn.gelu(response).astype(jnp.bfloat16)


def diagonal(blocks):
    groups, rows, columns = blocks.shape
    tiled = jnp.tile(blocks.reshape(groups * rows, columns), (1, groups))
    row = lax.broadcasted_iota(jnp.int32, tiled.shape, 0) // rows
    column = lax.broadcasted_iota(jnp.int32, tiled.shape, 1) // columns
    return split(jnp.where(row == column, tiled, 0.0))


def mixer(mixer_input, decay_shift, factors, readout_matrix, skip):
    factor_real, factor_imaginary, map_real, map_imaginary = factors
    rows, channels = mixer_input.shape
    groups, states = factor_real.shape
    width = groups * states

    def arrange(value):
        return jnp.swapaxes(value.reshape(LANES, rows // LANES, -1), 0, 1).reshape(rows, -1)

    values, shift = arrange(mixer_input), arrange(decay_shift)
    factor = jnp.stack([factor_real.reshape(width), factor_imaginary.reshape(width)])
    maps = jnp.stack(diagonal(map_real) + diagonal(map_imaginary))
    reads = jnp.stack(
        diagonal(readout_matrix[0]) + diagonal(readout_matrix[1])
    )
    vmem = pl.BlockSpec(memory_space=pltpu.VMEM)
    scratch = [pltpu.VMEM((rows, width), jnp.float32)] * 3
    parts, total = pl.pallas_call(
        totals_kernel,
        out_shape=(
            jax.ShapeDtypeStruct((4, LANES, width), jnp.float32),
            jax.ShapeDtypeStruct((LANES, width), jnp.float32),
        ),
        in_specs=[vmem] * 4,
        out_specs=(vmem, vmem),
        scratch_shapes=scratch,
        name="totals",
    )(values, shift, factor, maps)
    gathered = exchange(total, "sp", 0, gather=True)
    activated = pl.pallas_call(
        functools.partial(respond_kernel, "sp"),
        out_shape=jax.ShapeDtypeStruct((rows, channels), jnp.bfloat16),
        in_specs=[vmem] * 8,
        out_specs=vmem,
        scratch_shapes=scratch,
        name="respond",
    )(values, shift, factor, maps, parts, gathered, reads, skip.reshape(1, -1))
    return jnp.swapaxes(activated.reshape(rows // LANES, LANES, channels), 0, 1)


def slot_numbers(route_rows, experts, capacity):
    flat = route_rows.reshape(route_rows.shape[:-2] + (-1,))
    matches = (flat[..., None] == jnp.arange(experts, dtype=jnp.int32)).astype(jnp.int32)
    earlier = jnp.cumsum(matches, axis=-2) - matches
    return flat * capacity + jnp.sum(earlier * matches, axis=-1)


def dispatch_rows(slots, normed, width):
    hits = (slots[..., None] == jnp.arange(width, dtype=jnp.int32)).astype(jnp.bfloat16)
    tokens = normed.shape[-2]
    hits = hits.reshape(slots.shape[:-1] + (tokens, -1, width)).sum(axis=-2)
    return jnp.einsum(
        "...tw,...td->...wd", hits, normed, preferred_element_type=jnp.float32
    ).astype(jnp.bfloat16)


def shards(
    mixer_input,
    decay_shift,
    pole_real,
    pole_imaginary,
    log_step,
    input_map,
    readout_matrix,
    skip,
    out_proj,
    stream,
    norm_gain,
    routes,
    route_logits,
    w_gate,
    w_up,
    w_down,
):
    factors = discretize(pole_real, pole_imaginary, log_step, input_map)
    shares = lax.axis_size("tp")
    own_rows = stream.shape[0]
    activated = mixer(mixer_input, decay_shift, factors, readout_matrix, skip)
    whole_proj = lax.all_gather(out_proj, "tp", axis=0, tiled=True)
    received = exchange(activated.reshape(shares, own_rows, -1), "tp", 1)
    own_activated = jnp.swapaxes(received, 0, 1).reshape(own_rows, -1)
    projected = jnp.dot(own_activated, whole_proj, preferred_element_type=jnp.float32)
    mixed = (stream.astype(jnp.float32) + projected).astype(jnp.bfloat16)
    mixed_wide = mixed.astype(jnp.float32)
    normed = (
        mixed_wide
        * lax.rsqrt(jnp.mean(mixed_wide * mixed_wide, axis=-1, keepdims=True) + EPS)
        * norm_gain
    ).astype(jnp.bfloat16)
    weights = jax.nn.sigmoid(
        jnp.stack(
            [route_logits[:, 0] - route_logits[:, 1], route_logits[:, 1] - route_logits[:, 0]],
            axis=1,
        )
    )
    experts = lax.axis_size("sp") * w_gate.shape[0]
    capacity = 4 * own_rows // experts
    slot_width = experts * capacity
    model = stream.shape[1]
    own_slots = slot_numbers(routes, experts, capacity)
    outgoing = dispatch_rows(own_slots, normed, slot_width)
    arrived = exchange(outgoing.reshape(experts, capacity, model), "sp", 2)
    expert_rows = lax.all_gather(arrived.reshape(-1, model), "tp", axis=0, tiled=True)
    gate = jnp.dot(expert_rows, w_gate[0], preferred_element_type=jnp.float32)
    upward = jnp.dot(expert_rows, w_up[0], preferred_element_type=jnp.float32)
    hidden = (jax.nn.silu(gate) * upward).astype(jnp.bfloat16)
    summed = lax.psum_scatter(
        jnp.dot(hidden, w_down[0], preferred_element_type=jnp.float32).astype(jnp.bfloat16),
        "tp",
        scatter_dimension=0,
        tiled=True,
    )
    expert_out = summed.reshape(-1, capacity, model)
    returned_result = exchange(expert_out, "sp", 3).reshape(slot_width, model)
    picked = (
        jnp.take(returned_result, own_slots, axis=0)
        .astype(jnp.float32)
        .reshape(own_rows, -1, model)
    )
    combined = mixed_wide + jnp.sum(picked * weights[:, :, None], axis=1)
    return combined.astype(jnp.bfloat16)


def solution(mesh):
    return jax.shard_map(
        shards,
        mesh=mesh,
        in_specs=(
            P("sp", "tp"),
            P("sp", "tp"),
            P("tp", None),
            P("tp", None),
            P("tp"),
            P(None, "tp", None, None),
            P(None, "tp", None, None),
            P("tp"),
            P("tp", None),
            P(("sp", "tp"), None),
            P(),
            P(("sp", "tp"), None),
            P(("sp", "tp"), None),
            P("sp", None, "tp"),
            P("sp", None, "tp"),
            P("sp", "tp", None),
        ),
        out_specs=P(("sp", "tp"), None),
        check_vma=False,
    )
```

profile of v0, /device:TPU:8, one launch (start us, length us, event | category | flops | bytes accessed | tf_op | source)
XLA Modules:
  0.0 247.4 jit_solution(10290387214367177864)
XLA Ops:
  6.5 0.7 all-gather.3.cloned.1.call-update
  7.3 0.7 exp.17
  8.0 0.8 fusion.18
  9.0 1.0 fusion.29
  10.4 0.3 copy.58
  10.9 0.3 copy.59
  11.5 0.8 copy.55
  12.2 0.7 copy.73
  13.0 0.6 pad_maximum_fusion.2.factor
  13.6 0.9 select_convert_fusion.3
  14.5 0.9 subtract_convert_fusion.3
  15.4 1.6 pad_maximum_fusion.maps
  17.0 5.2 %totals.1 = (f32[4,8,1024]{2,1,0:T(8,128)}, f32[8,1024]{1,0:T(8,128)}) custom-call(bf16[256,256]{1,0:T(8,128)(2,1)} %bitcast.79, f32[256,16]{1,0:T(8,128)} %bitcast.77, f32[2,1024]{1,0:T(2,128)} %pad_maximum_fusion.2.factor, bf16[4,1024,256]{2,1,0:T(8,128)(2,1)} %pad_maximum_fusion.maps), custom_call_target="tpu_custom_call" | custom-call | tf_op jit(solution)/shard_map/totals/pallas_call | solution.py:236
  22.2 11.1 %exchange_0.1.gathered = f32[8,8,1024]{2,1,0:T(8,128)} custom-call(f32[8,1024]{1,0:T(8,128)} %get-tuple-element.8.value), custom_call_target="tpu_custom_call" | custom-call | tf_op jit(solution)/shard_map/exchange_0/pallas_call | solution.py:74
  33.6 0.3 copy.61
  35.0 1.6 pad_maximum_fusion.1.reads
  36.6 6.5 %respond.1 = bf16[256,256]{1,0:T(8,128)(2,1)} custom-call(bf16[256,256]{1,0:T(8,128)(2,1)} %bitcast.80, f32[256,16]{1,0:T(8,128)} %bitcast.78, f32[2,1024]{1,0:T(2,128)} %pad_maximum_fusion.2.factor, bf16[4,1024,256]{2,1,0:T(8,128)(2,1)} %pad_maximum_fusion.maps, f32[4,8,1024]{2,1,0:T(8,128)} %get-tuple-element.7.parts, f32[8,8,1024]{2,1,0:T(8,128)} %exchange_0.1.gathered, ...), custom_call_target="tpu_custom_call" | custom-call | tf_op jit(solution)/shard_map/respond/pallas_call | solution.py:248
  43.0 1.6 copy.64
  44.6 5.7 %exchange_1.1 = bf16[4,64,256]{2,1,0:T(8,128)(2,1)} custom-call(bf16[4,64,256]{2,1,0:T(8,128)(2,1)} %bitcast.83), custom_call_target="tpu_custom_call" | custom-call | tf_op jit(solution)/shard_map/exchange_1/pallas_call | solution.py:74
  50.3 0.9 copy.71
  52.3 3.2 %multiply_reduce_fusion.1 = (f32[64]{0:T(128)S(1)}, f32[64,2048]{1,0:T(8,128)S(1)}) fusion(bf16[64,1024]{1,0:T(8,128)(2,1)S(1)} %bitcast.87, bf16[1024,2048]{1,0:T(8,128)(2,1)} %all-gather.3.cloned.1.call-done, bf16[64,2048]{1,0:T(8,128)(2,1)S(1)} %copy-done.1), kind=kOutput, calls=%fused_computation.29 | convolution fusion | flops 269221824 | bytes 5112064 | tf_op jit(solution)/shard_map/dot_general | solution.py:300
  55.5 1.5 convolution_convert_fusion
  57.0 29.0 %exchange_2.1 = bf16[8,32,2048]{2,1,0:T(8,128)(2,1)} custom-call(bf16[8,32,2048]{2,1,0:T(8,128)(2,1)} %bitcast.72), custom_call_target="tpu_custom_call" | custom-call | tf_op jit(solution)/shard_map/exchange_2/pallas_call | solution.py:74
  86.3 36.3 %all-gather.5.cloned.1.call-done = bf16[1024,2048]{1,0:T(8,128)(2,1)} async-done(((bf16[256,2048]{1,0:T(8,128)(2,1)}), bf16[1024,2048]{1,0:T(8,128)(2,1)}) %all-gather.5.cloned.1.call-update) | async-done | bytes 4194320 | tf_op jit(solution)/shard_map/all_gather | solution.py:321
  122.5 13.5 %fusion.4 = f32[1024,1792]{1,0:T(8,128)} fusion(bf16[1024,2048]{1,0:T(8,128)(2,1)} %all-gather.5.cloned.1.call-done, bf16[1,2048,1792]{2,1,0:T(8,128)(2,1)} %param.29), kind=kOutput, calls=%fused_computation.5 | convolution fusion | flops 7516192768 | bytes 18874368 | tf_op jit(solution)/shard_map/dot_general | solution.py:322
  136.0 25.8 %fusion.8 = bf16[1024,2048]{1,0:T(8,128)(2,1)} fusion(bf16[1,1792,2048]{2,1,0:T(8,128)(2,1)} %param.31, f32[1024,1792]{1,0:T(8,128)} %fusion.4, bf16[1024,2048]{1,0:T(8,128)(2,1)} %all-gather.5.cloned.1.call-done, bf16[1,2048,1792]{2,1,0:T(8,128)(2,1)} %param.30), kind=kOutput, calls=%fused_computation.8 | convolution fusion | flops 15045492736 | bytes 30408704 | tf_op jit(solution)/shard_map/dot_general | solution.py:326
  162.7 44.0 %reduce-scatter.2.cloned.1.call-done = bf16[256,2048]{1,0:T(8,128)(2,1)} async-done(((bf16[1024,2048]{1,0:T(8,128)(2,1)}), bf16[256,2048]{1,0:T(8,128)(2,1)}) %reduce-scatter.2.cloned.1.call-update) | async-done | bytes 1048592 | tf_op jit(solution)/shard_map/reduce_scatter | solution.py:325
  206.7 28.0 %exchange_3.1 = bf16[8,32,2048]{2,1,0:T(8,128)(2,1)} custom-call(bf16[8,32,2048]{2,1,0:T(8,128)(2,1)} %bitcast.81), custom_call_target="tpu_custom_call" | custom-call | tf_op jit(solution)/shard_map/exchange_3/pallas_call | solution.py:74
  234.6 2.8 %gather_fusion = bf16[128,2048]{1,0:T(8,128)(2,1)S(1)} fusion(bf16[256,2048]{1,0:T(8,128)(2,1)} %bitcast.70, s32[1024]{0:T(1024)S(1)} %pad_clamp_fusion), kind=kCustom, calls=%fused_computation | custom fusion | bytes 1049088 | tf_op jit(solution)/shard_map/jit(_take)/gather | solution.py:334
  237.4 0.3 gather.7
  237.8 2.3 multiply_reduce_fusion
  240.1 0.8 add_convert_fusion
  (63 shorter events, 4.2 us)
Async XLA Ops:
  6.5 45.8 %all-gather.3.cloned.1.call-start = ((), (), s32[]{:S(2)}) async-start(), calls=%async_computation.1 | async-start | bytes 5242880 | tf_op jit(solution)/shard_map/all_gather | solution.py:297
  7.3 4.1 %copy-start.3 = (f32[256,16]{0,1:T(8,128)S(1)}, f32[256,16]{0,1:T(8,128)}, u32[]{:S(2)}) copy-start(f32[256,16]{0,1:T(8,128)} %param.17) | copy-start | bytes 49156
  7.3 115.3 %all-gather.5.cloned.1.call-start = ((), (), s32[]{:S(2)}) async-start(), calls=%async_computation.2 | async-start | bytes 5242880 | tf_op jit(solution)/shard_map/all_gather | solution.py:321
  9.0 3.3 %copy-start.2 = (bf16[256,256]{1,0:T(8,128)(2,1)S(1)}, bf16[256,256]{1,0:T(8,128)(2,1)}, u32[]{:S(2)}) copy-start(bf16[256,256]{1,0:T(8,128)(2,1)} %param.16) | copy-start | bytes 393220
  15.4 17.9 %copy-start = (f32[2,16,16,64]{3,2,1,0:T(8,128)S(1)}, f32[2,16,16,64]{3,2,1,0:T(8,128)}, u32[]{:S(2)}) copy-start(f32[2,16,16,64]{3,2,1,0:T(8,128)} %param.22) | copy-start | bytes 393220
  35.0 16.3 %copy-start.4 = (s32[64,2]{0,1:T(2,128)S(1)}, s32[64,2]{0,1:T(2,128)}, u32[]{:S(2)}) copy-start(s32[64,2]{0,1:T(2,128)} %param.27) | copy-start | bytes 1540
  35.0 17.3 %copy-start.1 = (bf16[64,2048]{1,0:T(8,128)(2,1)S(1)}, bf16[64,2048]{1,0:T(8,128)(2,1)}, u32[]{:S(2)}) copy-start(bf16[64,2048]{1,0:T(8,128)(2,1)} %param.25) | copy-start | bytes 786436
  43.0 12.4 %copy-start.5 = (f32[2048]{0:T(1024)S(1)}, f32[2048]{0:T(1024)}, u32[]{:S(2)}) copy-start(f32[2048]{0:T(1024)} %param.26) | copy-start | bytes 24580
  86.0 120.6 %reduce-scatter.2.cloned.1.call-start = ((), (), s32[]{:S(2)}) async-start(), calls=%async_computation.3 | async-start | bytes 5242880 | tf_op jit(solution)/shard_map/reduce_scatter | solution.py:325
  161.8 0.7 copy-start.6
Sparse Core Ops, SparseCore 0:
  8.9 35.6 all-gather.2
  86.1 36.3 all-gather.4
  162.0 44.6 reduce-scatter.1
where the time goes:
time: 249 us; the launch traced here: 247 us
  Pallas kernels  85.4 us (34%)
  waiting for transfers between devices  81 us (33%)
  matrix products  44 us (18%)
  between operations  13.5 us (5%)
  local copies, waits for them, and re-layouts  12.6 us (5%)
  other arithmetic  10.6 us (4%)
    pallas_call x4, Pallas kernels, exchange(): pl.pallas_call(functools.partial(exchange_kernel, axis, gather), out_shap...  73.8 us
    reduce_scatter x1, waiting for transfers between devices, shards(): lax.psum_scatter(jnp.dot(hidden, w_down[0], preferred_element_type=jnp.fl...  44 us
    all_gather x1, waiting for transfers between devices, shards(): lax.all_gather(arrived.reshape(-1, model), 'tp', axis=0, tiled=True)  36.3 us
    dot_general x1, matrix products, shards(): jnp.dot(hidden, w_down[0], preferred_element_type=jnp.float32)  25.8 us
    dot_general x1, matrix products, shards(): gate = jnp.dot(expert_rows, w_gate[0], preferred_element_type=jnp.float32)  13.5 us
    pallas_call x1, Pallas kernels, mixer(): pl.pallas_call(functools.partial(respond_kernel, 'sp'), out_shape=jax.Sha...  6.46 us
    pallas_call x1, Pallas kernels, mixer(): pl.pallas_call(totals_kernel, out_shape=(jax.ShapeDtypeStruct((4, LANES,...  5.21 us
  transfers between devices with their start and end apart: 3, of which 2 were waited for; matrix products, arithmetic and copies ran while one was open for 7% of the time, Pallas kernels for 12%

commit v1 on v0

--- a/solution.py
+++ b/solution.py
@@ -270,6 +270,301 @@
     return jnp.einsum(
         "...tw,...td->...wd", hits, normed, preferred_element_type=jnp.float32
     ).astype(jnp.bfloat16)
+
+
+def flip(index, bits):
+    bit = 1
+    while bit <= bits:
+        if bits & bit:
+            index = index + bit - 2 * bit * (index // bit % 2)
+        bit *= 2
+    return index
+
+
+def shuffle(chunks):
+    return [chunk for chunk in range(chunks) if chunk != 1] + [1] if chunks > 1 else [0]
+
+
+def moe_kernel(
+    normed, mixed, routes, weights, w_gate, w_up, w_down, out,
+    gate, up, down, outgoing, rows, hidden, kept, given, from_core, to_y, from_y, back, returned,
+    load_sem, sp_send, sp_recv, y_send, y_recv, core_send, core_recv, far_send, far_recv,
+    rc_send, rc_recv, ry_send, ry_recv, rs_send, rs_recv,
+):
+    experts = sp_send.shape[0]
+    tokens, model = out.shape
+    capacity = outgoing.shape[0] // experts
+    chunks = rows.shape[0]
+    width = gate.shape[1]
+    place, share = lax.axis_index("sp"), lax.axis_index("tp")
+    partner, across_y = flip(share, 1), flip(share, 2)
+    tile, wide = 256, 512
+    started = []
+
+    loads = []
+    for step in range(width // tile):
+        columns = pl.ds(step * tile, tile)
+        for number, (source, target) in enumerate(((w_gate, gate), (w_up, up))):
+            loads.append(
+                pltpu.make_async_copy(
+                    source.at[:, columns], target.at[:, columns], load_sem.at[number, step]
+                )
+            )
+    for step in range(model // wide):
+        columns = pl.ds(step * wide, wide)
+        loads.append(
+            pltpu.make_async_copy(w_down.at[:, columns], down.at[:, columns], load_sem.at[2, step])
+        )
+    for load in loads:
+        load.start()
+
+    barrier = pltpu.get_barrier_semaphore()
+    for bits in range(1, experts):
+        pl.semaphore_signal(
+            barrier, inc=1, device_id={"sp": flip(place, bits)}, device_id_type=MESH
+        )
+    for peer in (partner, across_y):
+        pl.semaphore_signal(barrier, inc=1, device_id={"tp": peer}, device_id_type=MESH)
+
+    names = [flip(place, bits) for bits in range(experts)]
+    first, second = routes[0:1, :], routes[1:2, :]
+    named = jnp.concatenate(
+        [((first == name) | (second == name)).astype(jnp.float32) for name in names], axis=0
+    )
+    earlier = (
+        lax.broadcasted_iota(jnp.int32, (tokens, tokens), 0)
+        < lax.broadcasted_iota(jnp.int32, (tokens, tokens), 1)
+    ).astype(jnp.float32)
+    rank = jnp.dot(named, earlier, preferred_element_type=jnp.float32).astype(jnp.int32)
+    scale = jnp.concatenate(
+        [
+            jnp.where(first == name, weights[0:1, :], 0.0)
+            + jnp.where(second == name, weights[1:2, :], 0.0)
+            for name in names
+        ],
+        axis=0,
+    )
+    slot = lax.broadcasted_iota(jnp.int32, (capacity, tokens), 0)
+    hits = [
+        jnp.where(slot == rank[e : e + 1, :], named[e : e + 1, :], 0.0) for e in range(experts)
+    ]
+    combine = jnp.concatenate([hit * scale[e : e + 1, :] for e, hit in enumerate(hits)], axis=0)
+    outgoing[...] = jnp.dot(
+        jnp.concatenate(hits, axis=0).astype(jnp.bfloat16),
+        normed[...],
+        preferred_element_type=jnp.float32,
+    ).astype(jnp.bfloat16)
+    spot = (0, 2, 1, 3)
+
+    def at(bits, kind):
+        return rows.at[bits // 2, pl.ds((spot[kind] * 2 + bits % 2) * capacity, capacity)]
+
+    def remote(source, target, send, receive, peer):
+        copy = pltpu.make_async_remote_copy(
+            src_ref=source, dst_ref=target, send_sem=send, recv_sem=receive,
+            device_id=peer, device_id_type=MESH,
+        )
+        copy.start()
+        started.append(copy)
+        return copy
+
+    def mine(bits):
+        return outgoing.at[pl.ds(bits * capacity, capacity)]
+
+    pl.semaphore_wait(barrier, experts + 1)
+    arrivals, y_arrivals, core_arrivals, far_arrivals = {}, {}, {}, {}
+
+    def pass_on(bits):
+        source = mine(0) if bits == 0 else at(bits, 0)
+        y_arrivals[bits] = remote(
+            source, at(bits, 2), y_send.at[bits], y_recv.at[bits], {"tp": across_y}
+        )
+        core_arrivals[bits] = remote(
+            source, at(bits, 1), core_send.at[bits], core_recv.at[bits], {"tp": partner}
+        )
+
+    pass_on(0)
+    order = shuffle(chunks)
+    for chunk in order:
+        for bits in (2 * chunk, 2 * chunk + 1):
+            if bits:
+                arrivals[bits] = remote(
+                    mine(bits), at(bits, 0), sp_send.at[bits], sp_recv.at[bits],
+                    {"sp": names[bits]},
+                )
+    rows[0, 0:capacity, :] = outgoing[0:capacity, :]
+
+    def relay(chunk):
+        for bits in (2 * chunk, 2 * chunk + 1):
+            if bits:
+                arrivals[bits].wait_recv()
+                pass_on(bits)
+
+    def relay_far(chunk):
+        for bits in (2 * chunk, 2 * chunk + 1):
+            y_arrivals[bits].wait_recv()
+            far_arrivals[bits] = remote(
+                at(bits, 2), at(bits, 3), far_send.at[bits], far_recv.at[bits], {"tp": partner}
+            )
+
+    def ready(chunk):
+        for bits in (2 * chunk, 2 * chunk + 1):
+            core_arrivals[bits].wait_recv()
+            far_arrivals[bits].wait_recv()
+
+    def widen(chunk, low, high, load):
+        def body(step, carry):
+            columns = pl.ds(pl.multiple_of(step * tile, tile), tile)
+            if load:
+                for number, (source, target) in enumerate(((w_gate, gate), (w_up, up))):
+                    pltpu.make_async_copy(
+                        source.at[:, columns], target.at[:, columns], load_sem.at[number, step]
+                    ).wait()
+            value = rows[chunk]
+            opened = jnp.dot(value, gate[:, columns], preferred_element_type=jnp.float32)
+            raised = jnp.dot(value, up[:, columns], preferred_element_type=jnp.float32)
+            hidden[:, columns] = (jax.nn.silu(opened) * raised).astype(jnp.bfloat16)
+            return carry
+
+        lax.fori_loop(low, high, body, 0)
+
+    half = rows.shape[1] // 2
+    quarter = half // 2
+
+    def narrow(chunk, load):
+        def body(step, carry):
+            columns = pl.ds(pl.multiple_of(step * wide, wide), wide)
+            if load:
+                pltpu.make_async_copy(
+                    w_down.at[:, columns], down.at[:, columns], load_sem.at[2, step]
+                ).wait()
+            value = jnp.dot(hidden[...], down[:, columns], preferred_element_type=jnp.float32)
+            kept[chunk, :, columns] = value[:half]
+            given[chunk, :, columns] = value[half:].astype(jnp.bfloat16)
+            return carry
+
+        lax.fori_loop(0, model // wide, body, 0)
+
+    core_back, y_back, sp_back = {}, {}, {}
+
+    def give(chunk):
+        core_back[chunk] = remote(
+            given.at[chunk], from_core.at[chunk], rc_send.at[chunk], rc_recv.at[chunk],
+            {"tp": partner},
+        )
+
+    def cross(chunk):
+        core_back[chunk].wait_recv()
+        to_y[chunk] = (
+            kept[chunk, quarter:, :] + from_core[chunk, quarter:, :].astype(jnp.float32)
+        ).astype(jnp.bfloat16)
+        y_back[chunk] = remote(
+            to_y.at[chunk], from_y.at[chunk], ry_send.at[chunk], ry_recv.at[chunk],
+            {"tp": across_y},
+        )
+
+    def give_back(chunk):
+        y_back[chunk].wait_recv()
+        total = (
+            kept[chunk, :quarter, :]
+            + from_core[chunk, :quarter, :].astype(jnp.float32)
+            + from_y[chunk].astype(jnp.float32)
+        ).astype(jnp.bfloat16)
+        back[chunk] = total
+        for side in range(2):
+            bits = 2 * chunk + side
+            span = pl.ds(side * capacity, capacity)
+            if bits:
+                sp_back[bits] = remote(
+                    back.at[chunk, span], returned.at[pl.ds(bits * capacity, capacity)],
+                    rs_send.at[bits], rs_recv.at[bits], {"sp": names[bits]},
+                )
+            else:
+                returned[0:capacity, :] = total[:capacity]
+
+    relay(0)
+    relay_far(0)
+    ready(0)
+    steps = width // tile
+    middle = (steps + 1) // 2
+    for number, chunk in enumerate(order):
+        later = order[number + 1] if number + 1 < chunks else None
+        before = order[number - 1] if number else None
+        widen(chunk, 0, middle, number == 0)
+        if later is not None:
+            relay(later)
+        if before is not None:
+            cross(before)
+        widen(chunk, middle, steps, number == 0)
+        if later is not None:
+            relay_far(later)
+        if before is not None:
+            give_back(before)
+        narrow(chunk, number == 0)
+        give(chunk)
+        if later is not None:
+            ready(later)
+    cross(order[-1])
+    give_back(order[-1])
+    for bits in range(1, experts):
+        sp_back[bits].wait_recv()
+    high, low = split(combine)
+    total = mixed[...].astype(jnp.float32)
+    for piece in (high, low):
+        total += lax.dot_general(
+            piece, returned[...], (((0,), (0,)), ((), ())), preferred_element_type=jnp.float32
+        )
+    out[...] = total.astype(jnp.bfloat16)
+    for copy in started:
+        copy.wait_send()
+
+
+def fits(shares, experts, capacity, w_gate):
+    if shares != 4 or w_gate.shape[0] != 1 or experts % 2 or experts & (experts - 1):
+        return False
+    return capacity % 16 == 0 and w_gate.shape[2] % 256 == 0 and w_gate.shape[1] % 512 == 0
+
+
+def moe(normed, mixed, routes, weights, w_gate, w_up, w_down, number):
+    tokens, model = normed.shape
+    experts, shares = lax.axis_size("sp"), lax.axis_size("tp")
+    capacity = 4 * tokens // experts
+    width = w_gate.shape[1]
+    slots, chunks = experts * capacity, experts // 2
+    group = 2 * shares * capacity
+    bf16, f32 = jnp.bfloat16, jnp.float32
+    vmem, anywhere = pl.BlockSpec(memory_space=pltpu.VMEM), pl.BlockSpec(memory_space=pl.ANY)
+    steps = max(width // 256, model // 512)
+    dma = pltpu.SemaphoreType.DMA
+    return pl.pallas_call(
+        moe_kernel,
+        out_shape=jax.ShapeDtypeStruct((tokens, model), bf16),
+        in_specs=[vmem] * 4 + [anywhere] * 3,
+        out_specs=vmem,
+        scratch_shapes=[
+            pltpu.VMEM((model, width), bf16),
+            pltpu.VMEM((model, width), bf16),
+            pltpu.VMEM((width, model), bf16),
+            pltpu.VMEM((slots, model), bf16),
+            pltpu.VMEM((chunks, group, model), bf16),
+            pltpu.VMEM((group, width), bf16),
+            pltpu.VMEM((chunks, group // 2, model), f32),
+            pltpu.VMEM((chunks, group // 2, model), bf16),
+            pltpu.VMEM((chunks, group // 2, model), bf16),
+            pltpu.VMEM((chunks, group // 4, model), bf16),
+            pltpu.VMEM((chunks, group // 4, model), bf16),
+            pltpu.VMEM((chunks, group // 4, model), bf16),
+            pltpu.VMEM((slots, model), bf16),
+            dma((3, steps)),
+        ]
+        + [dma((experts,))] * 8
+        + [dma((chunks,))] * 4
+        + [dma((experts,))] * 2,
+        compiler_params=pltpu.CompilerParams(
+            collective_id=number, has_side_effects=True, vmem_limit_bytes=62 * 2**20
+        ),
+        name="experts",
+    )(normed, mixed, routes, weights, w_gate, w_up, w_down)
 
 
 def shards(
@@ -313,6 +608,10 @@
     )
     experts = lax.axis_size("sp") * w_gate.shape[0]
     capacity = 4 * own_rows // experts
+    if fits(shares, experts, capacity, w_gate):
+        return moe(
+            normed, mixed, routes.T, weights.T, w_gate[0], w_up[0], w_down[0], 2
+        )
     slot_width = experts * capacity
     model = stream.shape[1]
     own_slots = slot_numbers(routes, experts, capacity)

time: 249 us -> 164 us (0.66)
  waiting for transfers between devices: 81 us -> 0.71 us
  matrix products: 44 us -> 3.18 us
  Pallas kernels: 85.4 us -> 126 us
  local copies, waits for them, and re-layouts: 12.6 us -> 9.99 us
    pallas_call x0 -> x1, Pallas kernels: none -> 97 us  [moe(): pl.pallas_call(moe_kernel, out_shape=jax.ShapeDtypeStruct((tokens, model)...]
    pallas_call x4 -> x2, Pallas kernels: 73.8 us -> 16.8 us  [exchange(): pl.pallas_call(functools.partial(exchange_kernel, axis, gather), out_shap...]
    reduce_scatter x1 -> x0, waiting for transfers between devices: 44 us -> none  [shards(): lax.psum_scatter(jnp.dot(hidden, w_down[0], preferred_element_type=jnp.fl...]
    dot_general x3 -> x0, matrix products: 40.8 us -> none  [the longest x1 25.8 us: shards(): jnp.dot(hidden, w_down[0], preferred_element_type=jnp.float32)]
    all_gather x1 -> x0, waiting for transfers between devices: 36.3 us -> none  [shards(): lax.all_gather(arrived.reshape(-1, model), 'tp', axis=0, tiled=True)]
    gather x2 -> x0, local copies, waits for them, and re-layouts: 3.14 us -> none  [shards(): jnp.take(returned_result, own_slots, axis=0).astype(jnp.float32)]
    reduce_sum x3 -> x0, other arithmetic: 2.59 us -> none  [the longest x1 2.33 us: shards(): combined = mixed_wide + jnp.sum(picked * weights[:, :, None], axis=1)]
  transfers between devices with their start and end apart: 3 -> 1, of which waited for: 2 -> 0; matrix products, arithmetic and copies ran while one was open for 7% -> 10% of each run, Pallas kernels for 12% -> 18%
where the time goes in v1:
time: 164 us; the launch traced here: 162 us
  Pallas kernels  126 us (77%)
  between operations  13.6 us (8%)
  local copies, waits for them, and re-layouts  9.99 us (6%)
  other arithmetic  8.44 us (5%)
  matrix products  3.18 us (2%)
    pallas_call x1, Pallas kernels, moe(): pl.pallas_call(moe_kernel, out_shape=jax.ShapeDtypeStruct((tokens, model)...  97 us
    pallas_call x2, Pallas kernels, exchange(): pl.pallas_call(functools.partial(exchange_kernel, axis, gather), out_shap...  16.8 us
    pallas_call x1, Pallas kernels, mixer(): pl.pallas_call(functools.partial(respond_kernel, 'sp'), out_shape=jax.Sha...  6.53 us
    pallas_call x1, Pallas kernels, mixer(): pl.pallas_call(totals_kernel, out_shape=(jax.ShapeDtypeStruct((4, LANES,...  5.27 us
  transfers between devices with their start and end apart: 1, of which 0 were waited for; matrix products, arithmetic and copies ran while one was open for 10% of the time, Pallas kernels for 18%

profile of v1, /device:TPU:8, one launch (start us, length us, event | category | flops | bytes accessed | tf_op | source)
XLA Modules:
  0.0 161.5 jit_solution(4532555329761631498)
XLA Ops:
  6.5 0.7 all-gather.2.cloned.1.call-update
  7.3 0.7 exp.9
  7.9 0.8 fusion.4
  8.9 1.0 fusion.13
  9.9 0.1 squeeze.10
  10.1 0.1 squeeze.22
  10.2 0.1 tile.36
  10.3 0.3 copy.24
  10.7 0.1 tile.38
  10.8 0.3 copy.25
  11.5 0.8 copy.21
  12.2 0.7 copy.34
  13.0 0.6 pad_maximum_fusion.2.factor
  13.6 0.9 select_convert_fusion.3
  14.5 0.9 subtract_convert_fusion.3
  15.4 1.6 %pad_maximum_fusion.maps = bf16[4,1024,256]{2,1,0:T(8,128)(2,1)} fusion(bf16[1,1024,256]{2,1,0:T(8,128)(2,1)S(1)} %get-tuple-element.26, bf16[1,1024,256]{2,1,0:T(8,128)(2,1)S(1)} %get-tuple-element.24, bf16[1,1024,256]{2,1,0:T(8,128)(2,1)S(1)} %get-tuple-element.25, bf16[1,1024,256]{2,1,0:T(8,128)(2,1)S(1)} %get-tuple-element.23), kind=kLoop, calls=%fused_computation.2 | loop fusion | flops 3145728 | bytes 4194304 | tf_op jit(solution)/shard_map/stack | solution.py:230
  17.0 5.3 %totals.1 = (f32[4,8,1024]{2,1,0:T(8,128)}, f32[8,1024]{1,0:T(8,128)}) custom-call(bf16[256,256]{1,0:T(8,128)(2,1)} %bitcast.50, f32[256,16]{1,0:T(8,128)} %bitcast.48, f32[2,1024]{1,0:T(2,128)} %pad_maximum_fusion.2.factor, bf16[4,1024,256]{2,1,0:T(8,128)(2,1)} %pad_maximum_fusion.maps), custom_call_target="tpu_custom_call" | custom-call | tf_op jit(solution)/shard_map/totals/pallas_call | solution.py:236
  22.3 11.1 %exchange_0.1.gathered = f32[8,8,1024]{2,1,0:T(8,128)} custom-call(f32[8,1024]{1,0:T(8,128)} %get-tuple-element.8.value), custom_call_target="tpu_custom_call" | custom-call | tf_op jit(solution)/shard_map/exchange_0/pallas_call | solution.py:74
  33.6 0.3 copy.27
  34.1 0.3 copy.29
  34.5 0.2 select_convert_fusion.1
  34.7 0.3 subtract_convert_fusion.1
  35.0 1.6 %pad_maximum_fusion.1.reads = bf16[4,256,1024]{2,1,0:T(8,128)(2,1)} fusion(bf16[1,256,1024]{2,1,0:T(8,128)(2,1)S(1)} %get-tuple-element.22, bf16[1,256,1024]{2,1,0:T(8,128)(2,1)S(1)} %get-tuple-element.20, bf16[1,256,1024]{2,1,0:T(8,128)(2,1)S(1)} %get-tuple-element.21, bf16[1,256,1024]{2,1,0:T(8,128)(2,1)S(1)} %get-tuple-element.19), kind=kLoop, calls=%fused_computation.3 | loop fusion | flops 3145728 | bytes 4194304 | tf_op jit(solution)/shard_map/stack | solution.py:231
  36.6 6.5 %respond.1 = bf16[256,256]{1,0:T(8,128)(2,1)} custom-call(bf16[256,256]{1,0:T(8,128)(2,1)} %bitcast.51, f32[256,16]{1,0:T(8,128)} %bitcast.49, f32[2,1024]{1,0:T(2,128)} %pad_maximum_fusion.2.factor, bf16[4,1024,256]{2,1,0:T(8,128)(2,1)} %pad_maximum_fusion.maps, f32[4,8,1024]{2,1,0:T(8,128)} %get-tuple-element.7.parts, f32[8,8,1024]{2,1,0:T(8,128)} %exchange_0.1.gathered, ...), custom_call_target="tpu_custom_call" | custom-call | tf_op jit(solution)/shard_map/respond/pallas_call | solution.py:248
  43.1 1.6 copy.30
  44.7 5.7 %exchange_1.1 = bf16[4,64,256]{2,1,0:T(8,128)(2,1)} custom-call(bf16[4,64,256]{2,1,0:T(8,128)(2,1)} %bitcast.54), custom_call_target="tpu_custom_call" | custom-call | tf_op jit(solution)/shard_map/exchange_1/pallas_call | solution.py:74
  50.4 0.9 copy.32
  51.4 0.6 fusion.11.weights
  52.0 3.2 %fusion.1 = (f32[64]{0:T(128)S(1)}, bf16[64,2048]{1,0:T(8,128)(2,1)S(1)}) fusion(bf16[64,1024]{1,0:T(8,128)(2,1)S(1)} %bitcast.52, bf16[1024,2048]{1,0:T(8,128)(2,1)} %all-gather.2.cloned.1.call-done, bf16[64,2048]{1,0:T(8,128)(2,1)S(1)} %copy-done.1), kind=kOutput, calls=%fused_computation.16 | convolution fusion | flops 269221824 | bytes 4849920 | tf_op jit(solution)/shard_map/dot_general | solution.py:595
  55.2 0.8 fusion.3.normed
  56.0 97.0 %experts.1 = bf16[64,2048]{1,0:T(8,128)(2,1)} custom-call(bf16[64,2048]{1,0:T(8,128)(2,1)} %fusion.3.normed, bf16[64,2048]{1,0:T(8,128)(2,1)} %copy-done, s32[2,64]{1,0:T(2,128)} %bitcast.59, f32[2,64]{1,0:T(2,128)} %fusion.11.weights, bf16[2048,1792]{1,0:T(8,128)(2,1)} %bitcast.41, bf16[2048,1792]{1,0:T(8,128)(2,1)} %bitcast.42, bf16[1792,2048]{1,0:T(8,128)(2,1)} %bitcast.43), custom_call_target="tpu_custom_call" | custom-call | tf_op jit(solution)/shard_map/experts/pallas_call | solution.py:539
  153.0 1.7 %copy.36 = bf16[64,2048]{1,0:T(8,128)(2,1)} copy(bf16[64,2048]{1,0:T(8,128)(2,1)} %experts.1) | data formatting | bytes 524288
  (35 shorter events, 1.0 us)
Async XLA Ops:
  6.5 45.4 %all-gather.2.cloned.1.call-start = ((), (), s32[]{:S(2)}) async-start(), calls=%async_computation | async-start | bytes 5242880 | tf_op jit(solution)/shard_map/all_gather | solution.py:592
  10.7 0.7 copy-start.4
  10.7 1.6 copy-start.3
  17.0 16.4 %copy-start.2 = (f32[2,16,16,64]{3,2,1,0:T(8,128)S(1)}, f32[2,16,16,64]{3,2,1,0:T(8,128)}, u32[]{:S(2)}) copy-start(f32[2,16,16,64]{3,2,1,0:T(8,128)} %param.22) | copy-start | bytes 393220
  36.6 14.7 %copy-start.6 = (f32[64,2]{0,1:T(2,128)S(1)}, f32[64,2]{0,1:T(2,128)}, u32[]{:S(2)}) copy-start(f32[64,2]{0,1:T(2,128)} %param.28) | copy-start | bytes 1540
  36.6 15.3 %copy-start.1 = (bf16[64,2048]{1,0:T(8,128)(2,1)S(1)}, bf16[64,2048]{1,0:T(8,128)(2,1)}, u32[]{:S(2)}) copy-start(bf16[64,2048]{1,0:T(8,128)(2,1)} %param.25) | copy-start | bytes 786436
  52.0 3.2 %copy-start.5 = (f32[2048]{0:T(1024)S(1)}, f32[2048]{0:T(1024)}, u32[]{:S(2)}) copy-start(f32[2048]{0:T(1024)} %param.26) | copy-start | bytes 24580
  55.1 0.9 copy-start
Sparse Core Ops, SparseCore 0:
  8.9 35.6 all-gather.1

commit v2 on v0

--- a/solution.py
+++ b/solution.py
@@ -272,6 +272,561 @@
     ).astype(jnp.bfloat16)
 
 
+def flip(index, bits):
+    bit = 1
+    while bit <= bits:
+        if bits & bit:
+            index = index + bit - 2 * bit * (index // bit % 2)
+        bit *= 2
+    return index
+
+
+def plan(experts):
+    if experts == 8:
+        order, sends = (0, 1, 4, 2, 5, 6, 7, 3), (1, 4, 2, 5, 6, 7, 3)
+        near, far = (0, 0, 0, 1, 6, 12, 15, 17), (0, 0, 5, 7, 12, 17, 20, 23)
+    else:
+        order, sends = tuple(range(experts)), tuple(range(1, experts))
+        near = tuple(max(0, 4 * place - 12) for place in range(experts))
+        far = tuple(max(0, 4 * place - 6) for place in range(experts))
+    events = {slot: [] for slot in range(4 * experts)}
+    for place in range(experts):
+        if place > 1:
+            events[near[place]].append(("pass_on", order[place]))
+        if place > 0:
+            events[far[place]].append(("pass_far", order[place]))
+    late = []
+    for place in range(experts):
+        for name, slot in (("cross", 4 * place + 5), ("give_back", 4 * place + 10)):
+            if slot < 4 * experts:
+                events[slot].append((name, order[place]))
+            else:
+                late.append((slot, name, order[place]))
+    return order, sends, events, [item[1:] for item in sorted(late)]
+
+
+def moe_kernel(
+    normed, mixed, routes, weights, w_gate, w_up, w_down, out,
+    gate, up, down, outgoing, rows, hidden, kept, given, from_core, to_y, from_y, back, returned,
+    load_sem, send_sem, recv_sem,
+):
+    experts = rows.shape[0]
+    tokens, model = out.shape
+    capacity = outgoing.shape[1]
+    width = gate.shape[1]
+    tile, wide = width // 2, model // 2
+    place, share = lax.axis_index("sp"), lax.axis_index("tp")
+    partner, across_y = flip(share, 1), flip(share, 2)
+    names = [flip(place, bits) for bits in range(experts)]
+    order, sends, events, late = plan(experts)
+
+    def load(number, step):
+        source, target = ((w_gate, gate), (w_up, up), (w_down, down))[number]
+        length = wide if number == 2 else tile
+        columns = pl.ds(pl.multiple_of(step * length, 128), length)
+        return pltpu.make_async_copy(
+            source.at[:, columns], target.at[:, columns], load_sem.at[number, step]
+        )
+
+    for step in range(2):
+        load(0, step).start()
+        load(1, step).start()
+    for step in range(2):
+        load(2, step).start()
+
+    barrier = pltpu.get_barrier_semaphore()
+    for bits in range(1, experts):
+        pl.semaphore_signal(barrier, inc=1, device_id={"sp": names[bits]}, device_id_type=MESH)
+    for peer in (partner, across_y):
+        pl.semaphore_signal(barrier, inc=1, device_id={"tp": peer}, device_id_type=MESH)
+
+    first, second = routes[0:1, :], routes[1:2, :]
+    named = jnp.concatenate(
+        [((first == name) | (second == name)).astype(jnp.float32) for name in names], axis=0
+    )
+    earlier = (
+        lax.broadcasted_iota(jnp.int32, (tokens, tokens), 0)
+        < lax.broadcasted_iota(jnp.int32, (tokens, tokens), 1)
+    ).astype(jnp.float32)
+    rank = jnp.dot(named, earlier, preferred_element_type=jnp.float32).astype(jnp.int32)
+    scale = jnp.concatenate(
+        [
+            jnp.where(first == name, weights[0:1, :], 0.0)
+            + jnp.where(second == name, weights[1:2, :], 0.0)
+            for name in names
+        ],
+        axis=0,
+    )
+    slot = lax.broadcasted_iota(jnp.int32, (capacity, tokens), 0)
+    hits = [
+        jnp.where(slot == rank[e : e + 1, :], named[e : e + 1, :], 0.0) for e in range(experts)
+    ]
+    combine = jnp.concatenate([hit * scale[e : e + 1, :] for e, hit in enumerate(hits)], axis=0)
+    outgoing[...] = (
+        jnp.dot(
+            jnp.concatenate(hits, axis=0).astype(jnp.bfloat16),
+            normed[...],
+            preferred_element_type=jnp.float32,
+        )
+        .astype(jnp.bfloat16)
+        .reshape(outgoing.shape)
+    )
+    spot = (0, 2, 1, 3)
+
+    def at(bits, kind):
+        return rows.at[bits, pl.ds(spot[kind] * capacity, capacity)]
+
+    def remote(kind, bits):
+        source, target, peer = {
+            "sp": lambda: (outgoing.at[bits], at(bits, 0), {"sp": names[bits]}),
+            "y": lambda: (at(bits, 0), at(bits, 2), {"tp": across_y}),
+            "core": lambda: (at(bits, 0), at(bits, 1), {"tp": partner}),
+            "far": lambda: (at(bits, 2), at(bits, 3), {"tp": partner}),
+            "core_back": lambda: (given.at[bits], from_core.at[bits], {"tp": partner}),
+            "y_back": lambda: (to_y.at[bits], from_y.at[bits], {"tp": across_y}),
+            "sp_back": lambda: (back.at[bits], returned.at[bits], {"sp": names[bits]}),
+        }[kind]()
+        if bits == 0 and kind in ("y", "core"):
+            source = outgoing.at[0]
+        number = KINDS.index(kind)
+        return pltpu.make_async_remote_copy(
+            src_ref=source, dst_ref=target,
+            send_sem=send_sem.at[number, bits], recv_sem=recv_sem.at[number, bits],
+            device_id=peer, device_id_type=MESH,
+        )
+
+    def pass_on(bits):
+        if bits:
+            remote("sp", bits).wait_recv()
+        remote("y", bits).start()
+        remote("core", bits).start()
+
+    def pass_far(bits):
+        remote("y", bits).wait_recv()
+        remote("far", bits).start()
+
+    def cross(bits):
+        remote("core_back", bits).wait_recv()
+        to_y[bits] = (
+            kept[bits, capacity:, :] + from_core[bits, capacity:, :].astype(jnp.float32)
+        ).astype(jnp.bfloat16)
+        remote("y_back", bits).start()
+
+    def give_back(bits):
+        remote("y_back", bits).wait_recv()
+        total = (
+            kept[bits, :capacity, :]
+            + from_core[bits, :capacity, :].astype(jnp.float32)
+            + from_y[bits].astype(jnp.float32)
+        ).astype(jnp.bfloat16)
+        if bits:
+            back[bits] = total
+            remote("sp_back", bits).start()
+        else:
+            returned[0] = total
+
+    acts = {"pass_on": pass_on, "pass_far": pass_far, "cross": cross, "give_back": give_back}
+
+    def act(step, slots):
+        for number, slot in enumerate(slots):
+            if events[slot]:
+                @pl.when(step == number)
+                def _():
+                    for name, bits in events[slot]:
+                        acts[name](bits)
+
+    pl.semaphore_wait(barrier, experts + 1)
+    pass_on(0)
+    for bits in sends:
+        remote("sp", bits).start()
+    rows[0, 0:capacity, :] = outgoing[0]
+    pass_on(order[1])
+    pass_far(0)
+    for number, bits in enumerate(order):
+        remote("core", bits).wait_recv()
+        remote("far", bits).wait_recv()
+
+        def widen(step, carry):
+            columns = pl.ds(pl.multiple_of(step * tile, 128), tile)
+            if number == 0:
+                load(0, step).wait()
+                load(1, step).wait()
+            value = rows[bits]
+            opened = jnp.dot(value, gate[:, columns], preferred_element_type=jnp.float32)
+            raised = jnp.dot(value, up[:, columns], preferred_element_type=jnp.float32)
+            hidden[:, columns] = (jax.nn.silu(opened) * raised).astype(jnp.bfloat16)
+            act(step, (4 * number, 4 * number + 1))
+            return carry
+
+        lax.fori_loop(0, 2, widen, 0)
+
+        def narrow(step, carry):
+            columns = pl.ds(pl.multiple_of(step * wide, 128), wide)
+            if number == 0:
+                load(2, step).wait()
+            value = jnp.dot(hidden[...], down[:, columns], preferred_element_type=jnp.float32)
+            kept[bits, :, columns] = value[: 2 * capacity]
+            given[bits, :, columns] = value[2 * capacity :].astype(jnp.bfloat16)
+            act(step, (4 * number + 2, 4 * number + 3))
+            return carry
+
+        lax.fori_loop(0, 2, narrow, 0)
+        remote("core_back", bits).start()
+    for name, bits in late:
+        acts[name](bits)
+    for bits in sends:
+        remote("sp_back", bits).wait_recv()
+    total = mixed[...].astype(jnp.float32)
+    every = returned[...].reshape(experts * capacity, model)
+    for piece in split(combine):
+        total += lax.dot_general(
+            piece, every, (((0,), (0,)), ((), ())), preferred_element_type=jnp.float32
+        )
+    out[...] = total.astype(jnp.bfloat16)
+    for bits in range(experts):
+        for kind in KINDS:
+            if bits or kind not in ("sp", "sp_back"):
+                remote(kind, bits).wait_send()
+
+
+KINDS = ("sp", "y", "core", "far", "core_back", "y_back", "sp_back")
+
+
+def fits(shares, experts, capacity, w_gate):
+    if shares != 4 or w_gate.shape[0] != 1 or experts & (experts - 1) or experts < 2:
+        return False
+    return capacity % 16 == 0 and w_gate.shape[2] % 256 == 0 and w_gate.shape[1] % 256 == 0
+
+
+def moe(normed, mixed, routes, weights, w_gate, w_up, w_down, number):
+    tokens, model = normed.shape
+    experts = lax.axis_size("sp")
+    capacity = 4 * tokens // experts
+    width = w_gate.shape[1]
+    group = 4 * capacity
+    bf16, f32 = jnp.bfloat16, jnp.float32
+    vmem, anywhere = pl.BlockSpec(memory_space=pltpu.VMEM), pl.BlockSpec(memory_space=pl.ANY)
+    dma = pltpu.SemaphoreType.DMA
+    return pl.pallas_call(
+        moe_kernel,
+        out_shape=jax.ShapeDtypeStruct((tokens, model), bf16),
+        in_specs=[vmem] * 4 + [anywhere] * 3,
+        out_specs=vmem,
+        scratch_shapes=[
+            pltpu.VMEM((model, width), bf16),
+            pltpu.VMEM((model, width), bf16),
+            pltpu.VMEM((width, model), bf16),
+            pltpu.VMEM((experts, capacity, model), bf16),
+            pltpu.VMEM((experts, group, model), bf16),
+            pltpu.VMEM((group, width), bf16),
+            pltpu.VMEM((experts, 2 * capacity, model), f32),
+            pltpu.VMEM((experts, 2 * capacity, model), bf16),
+            pltpu.VMEM((experts, 2 * capacity, model), bf16),
+            pltpu.VMEM((experts, capacity, model), bf16),
+            pltpu.VMEM((experts, capacity, model), bf16),
+            pltpu.VMEM((experts, capacity, model), bf16),
+            pltpu.VMEM((experts, capacity, model), bf16),
+            dma((3, 2)),
+            dma((len(KINDS), experts)),
+            dma((len(KINDS), experts)),
+        ],
+        compiler_params=pltpu.CompilerParams(
+            collective_id=number, has_side_effects=True, vmem_limit_bytes=62 * 2**20
+        ),
+        name="experts",
+    )(normed, mixed, routes, weights, w_gate, w_up, w_down)
+
+
+def same(shape, row, column):
+    rows = lax.broadcasted_iota(jnp.int32, shape, 0)
+    columns = lax.broadcasted_iota(jnp.int32, shape, 1)
+    return row(rows) == column(columns)
+
+
+def chain(later, earlier):
+    b_real, b_imaginary, y_real, y_imaginary = later
+    a_real, a_imaginary, x_real, x_imaginary = earlier
+    return (
+        b_real * a_real - b_imaginary * a_imaginary,
+        b_real * a_imaginary + b_imaginary * a_real,
+        b_real * x_real - b_imaginary * x_imaginary + y_real,
+        b_real * x_imaginary + b_imaginary * x_real + y_imaginary,
+    )
+
+
+def mixer_kernel(
+    values, shift, pole_real, pole_imaginary, log_step, input_map, readout, skip, out_proj,
+    stream, gain, mixed, normed,
+    scale, drive_real, drive_imaginary, parts, total, gathered, activated, acts, proj,
+    sp_send, sp_recv, tp_send, tp_recv, proj_send, proj_recv,
+):
+    rows, width = scale.shape
+    groups, states = pole_real.shape
+    inner = input_map.shape[1]
+    channels = groups * inner
+    own_rows = mixed.shape[0]
+    count = lax.axis_size("sp")
+    place, share = lax.axis_index("sp"), lax.axis_index("tp")
+    partner, across_y = flip(share, 1), flip(share, 2)
+    float_dot = functools.partial(
+        jnp.dot, precision=TOP_PRECISION, preferred_element_type=jnp.float32
+    )
+    pieces = proj_send.shape[1]
+    depth = channels // pieces
+
+    barrier = pltpu.get_barrier_semaphore()
+    for bits in range(1, count):
+        pl.semaphore_signal(
+            barrier, inc=1, device_id={"sp": flip(place, bits)}, device_id_type=MESH
+        )
+    for kind in range(1, 4):
+        pl.semaphore_signal(
+            barrier, inc=1, device_id={"tp": flip(share, kind)}, device_id_type=MESH
+        )
+
+    def remote(source, target, send, receive, peer):
+        return pltpu.make_async_remote_copy(
+            src_ref=source, dst_ref=target, send_sem=send, recv_sem=receive,
+            device_id=peer, device_id_type=MESH,
+        )
+
+    def weights(kind, piece):
+        span = pl.ds(piece * depth, depth)
+        source = proj.at[2, span] if kind == 3 else out_proj.at[span]
+        peer = across_y if kind == 2 else partner
+        return remote(
+            source, proj.at[kind, span], proj_send.at[kind, piece], proj_recv.at[kind, piece],
+            {"tp": peer},
+        )
+
+    pl.semaphore_wait(barrier, count + 2)
+    for piece in range(pieces):
+        weights(2, piece).start()
+    for piece in range(pieces):
+        weights(1, piece).start()
+
+    spread = same((states, width), lambda r: r, lambda c: c % states).astype(jnp.float32)
+    group = same((groups, width), lambda r: r, lambda c: c // states)
+    stacked = jnp.concatenate(
+        [
+            pole_real[...],
+            pole_imaginary[...],
+            jnp.broadcast_to(log_step[...], (groups, states)),
+        ],
+        axis=0,
+    )
+    laid = float_dot(stacked, spread)
+    real, imaginary, logarithm = (
+        jnp.sum(
+            jnp.where(group, laid[n * groups : (n + 1) * groups], 0.0), axis=0, keepdims=True
+        )
+        for n in range(3)
+    )
+    step = jnp.exp(logarithm)
+    magnitude = jnp.exp(real * step)
+    factor_real = magnitude * jnp.cos(imaginary * step)
+    factor_imaginary = magnitude * jnp.sin(imaginary * step)
+    denominator = real * real + imaginary * imaginary
+    ratio_real = ((factor_real - 1.0) * real + factor_imaginary * imaginary) / denominator
+    ratio_imaginary = (factor_imaginary * real - (factor_real - 1.0) * imaginary) / denominator
+    map_real = ratio_real * input_map[0] - ratio_imaginary * input_map[1]
+    map_imaginary = ratio_real * input_map[1] + ratio_imaginary * input_map[0]
+
+    segment = rows // LANES
+    permute = same((rows, rows), lambda r: r % LANES * segment + r // LANES, lambda c: c)
+    entries = jnp.dot(
+        permute.astype(jnp.bfloat16), values[...], preferred_element_type=jnp.float32
+    ).astype(jnp.bfloat16)
+    growth = float_dot(permute.astype(jnp.float32), jnp.exp(shift[...]))
+    scale[...] = float_dot(growth, group.astype(jnp.float32))
+    block = same((channels, width), lambda r: r // inner, lambda c: c // states)
+
+    def diagonal(value):
+        return [
+            jnp.where(block, jnp.concatenate([piece] * groups, axis=0), 0.0).astype(jnp.bfloat16)
+            for piece in (part.astype(jnp.float32) for part in split(value))
+        ]
+
+    for target, value in ((drive_real, map_real), (drive_imaginary, map_imaginary)):
+        high, low = diagonal(value)
+        target[...] = jnp.dot(entries, high, preferred_element_type=jnp.float32) + jnp.dot(
+            entries, low, preferred_element_type=jnp.float32
+        )
+
+    wide = (LANES, width)
+    wide_real = jnp.broadcast_to(factor_real, wide)
+    wide_imaginary = jnp.broadcast_to(factor_imaginary, wide)
+
+    def first_pass(position, carry):
+        at = pl.ds(pl.multiple_of(position * LANES, LANES), LANES)
+        grow = scale[at, :]
+        item = (
+            grow * wide_real, grow * wide_imaginary, drive_real[at, :], drive_imaginary[at, :]
+        )
+        return chain(item, carry)
+
+    empty = jnp.zeros(wide, jnp.float32)
+    ends = lax.fori_loop(
+        0, segment, first_pass, (jnp.ones(wide, jnp.float32), empty, empty, empty)
+    )
+    for number, end in enumerate(ends):
+        parts[number] = end
+    run = tuple(end[0:1] for end in ends)
+    for number in range(1, LANES):
+        run = chain(tuple(end[number : number + 1] for end in ends), run)
+    total[...] = jnp.concatenate(run + (jnp.zeros((LANES - 4, width), jnp.float32),), axis=0)
+    gathered[place] = total[...]
+
+    def totals(bits):
+        return remote(
+            total, gathered.at[place], sp_send.at[bits], sp_recv.at[bits],
+            {"sp": flip(place, bits)},
+        )
+
+    for bits in range(1, count):
+        totals(bits).start()
+
+    spread_low = spread.astype(jnp.bfloat16)
+    reads = []
+    for number in range(2):
+        for piece in split(readout[number]):
+            tiled = jnp.dot(piece, spread_low, preferred_element_type=jnp.float32)
+            reads.append(jnp.where(block, tiled, 0.0).astype(jnp.bfloat16))
+    for bits in range(1, count):
+        totals(bits).wait_recv()
+
+    def before(position, carry):
+        real, imaginary = carry
+        item = gathered[position]
+        a_real, a_imaginary = item[0:1], item[1:2]
+        keep = position < place
+        return (
+            jnp.where(keep, a_real * real - a_imaginary * imaginary + item[2:3], real),
+            jnp.where(keep, a_real * imaginary + a_imaginary * real + item[3:4], imaginary),
+        )
+
+    none = jnp.zeros((1, width), jnp.float32)
+    real, imaginary = lax.fori_loop(0, count - 1, before, (none, none))
+    reals, imaginaries = [real], [imaginary]
+    for number in range(LANES - 1):
+        at = slice(number, number + 1)
+        a_real, a_imaginary = parts[0, at, :], parts[1, at, :]
+        real, imaginary = (
+            a_real * real - a_imaginary * imaginary + parts[2, at, :],
+            a_real * imaginary + a_imaginary * real + parts[3, at, :],
+        )
+        reals.append(real)
+        imaginaries.append(imaginary)
+
+    def second_pass(position, carry):
+        x_real, x_imaginary = carry
+        at = pl.ds(pl.multiple_of(position * LANES, LANES), LANES)
+        grow = scale[at, :]
+        b_real, b_imaginary = grow * wide_real, grow * wide_imaginary
+        new_real = b_real * x_real - b_imaginary * x_imaginary + drive_real[at, :]
+        new_imaginary = b_real * x_imaginary + b_imaginary * x_real + drive_imaginary[at, :]
+        drive_real[at, :] = new_real
+        drive_imaginary[at, :] = new_imaginary
+        return new_real, new_imaginary
+
+    lax.fori_loop(
+        0,
+        segment,
+        second_pass,
+        (jnp.concatenate(reals, axis=0), jnp.concatenate(imaginaries, axis=0)),
+    )
+    high, low = split(drive_real[...])
+    response = across(high, reads[0]) + across(low, reads[0]) + across(high, reads[1])
+    high, low = split(drive_imaginary[...])
+    response -= across(high, reads[2]) + across(low, reads[2]) + across(high, reads[3])
+    response += skip[...] * entries.astype(jnp.float32)
+    restore = same((rows, rows), lambda r: r, lambda c: c % LANES * segment + c // LANES)
+    activated[...] = jnp.dot(
+        restore.astype(jnp.bfloat16),
+        jax.nn.gelu(response).astype(jnp.bfloat16),
+        preferred_element_type=jnp.float32,
+    ).astype(jnp.bfloat16)
+
+    def hand(kind):
+        peer = flip(share, kind)
+        start = pl.multiple_of(peer * own_rows, own_rows)
+        return remote(
+            activated.at[pl.ds(start, own_rows)], acts.at[kind], tp_send.at[kind],
+            tp_recv.at[kind], {"tp": peer},
+        )
+
+    for kind in range(1, 4):
+        hand(kind).start()
+    acts[0] = activated[pl.ds(pl.multiple_of(share * own_rows, own_rows), own_rows), :]
+    for piece in range(pieces):
+        weights(2, piece).wait_recv()
+        weights(3, piece).start()
+    projected = jnp.dot(acts[0], out_proj[...], preferred_element_type=jnp.float32)
+    for kind in range(1, 4):
+        hand(kind).wait_recv()
+        for piece in range(pieces):
+            if kind != 2:
+                weights(kind, piece).wait_recv()
+        projected += jnp.dot(acts[kind], proj[kind], preferred_element_type=jnp.float32)
+    result = (stream[...].astype(jnp.float32) + projected).astype(jnp.bfloat16)
+    mixed[...] = result
+    broad = result.astype(jnp.float32)
+    normed[...] = (
+        broad * lax.rsqrt(jnp.mean(broad * broad, axis=-1, keepdims=True) + EPS) * gain[...]
+    ).astype(jnp.bfloat16)
+    for bits in range(1, count):
+        totals(bits).wait_send()
+    for kind in range(1, 4):
+        hand(kind).wait_send()
+        for piece in range(pieces):
+            weights(kind, piece).wait_send()
+
+
+def mixer_block(
+    mixer_input, decay_shift, pole_real, pole_imaginary, log_step, input_map, readout_matrix,
+    skip, out_proj, stream, norm_gain, number,
+):
+    rows, channels = mixer_input.shape
+    groups, states = pole_real.shape
+    width = groups * states
+    count = lax.axis_size("sp")
+    own_rows, model = stream.shape
+    bf16, f32 = jnp.bfloat16, jnp.float32
+    vmem = pl.BlockSpec(memory_space=pltpu.VMEM)
+    dma = pltpu.SemaphoreType.DMA
+    pieces = 2
+    turned = jnp.swapaxes(input_map.reshape(2, width, -1), 1, 2)
+    return pl.pallas_call(
+        mixer_kernel,
+        out_shape=(jax.ShapeDtypeStruct((own_rows, model), bf16),) * 2,
+        in_specs=[vmem] * 11,
+        out_specs=(vmem, vmem),
+        scratch_shapes=[pltpu.VMEM((rows, width), f32)] * 3
+        + [
+            pltpu.VMEM((4, LANES, width), f32),
+            pltpu.VMEM((LANES, width), f32),
+            pltpu.VMEM((count, LANES, width), f32),
+            pltpu.VMEM((rows, channels), bf16),
+            pltpu.VMEM((4, own_rows, channels), bf16),
+            pltpu.VMEM((4, channels, model), bf16),
+            dma((count,)),
+            dma((count,)),
+            dma((4,)),
+            dma((4,)),
+            dma((4, pieces)),
+            dma((4, pieces)),
+        ],
+        compiler_params=pltpu.CompilerParams(
+            collective_id=number, has_side_effects=True, vmem_limit_bytes=48 * 2**20
+        ),
+        name="mixer",
+    )(
+        mixer_input, decay_shift, pole_real, pole_imaginary, log_step.reshape(-1, 1), turned,
+        readout_matrix.reshape(2, channels, states), skip.reshape(1, -1), out_proj, stream,
+        norm_gain.reshape(1, -1),
+    )
+
+
 def shards(
     mixer_input,
     decay_shift,
@@ -290,9 +845,23 @@
     w_up,
     w_down,
 ):
-    factors = discretize(pole_real, pole_imaginary, log_step, input_map)
     shares = lax.axis_size("tp")
     own_rows = stream.shape[0]
+    weights = jax.nn.sigmoid(
+        jnp.stack(
+            [route_logits[:, 0] - route_logits[:, 1], route_logits[:, 1] - route_logits[:, 0]],
+            axis=1,
+        )
+    )
+    experts = lax.axis_size("sp") * w_gate.shape[0]
+    capacity = 4 * own_rows // experts
+    if fits(shares, experts, capacity, w_gate):
+        mixed, normed = mixer_block(
+            mixer_input, decay_shift, pole_real, pole_imaginary, log_step, input_map,
+            readout_matrix, skip, out_proj, stream, norm_gain, 1,
+        )
+        return moe(normed, mixed, routes.T, weights.T, w_gate[0], w_up[0], w_down[0], 2)
+    factors = discretize(pole_real, pole_imaginary, log_step, input_map)
     activated = mixer(mixer_input, decay_shift, factors, readout_matrix, skip)
     whole_proj = lax.all_gather(out_proj, "tp", axis=0, tiled=True)
     received = exchange(activated.reshape(shares, own_rows, -1), "tp", 1)
@@ -305,14 +874,6 @@
         * lax.rsqrt(jnp.mean(mixed_wide * mixed_wide, axis=-1, keepdims=True) + EPS)
         * norm_gain
     ).astype(jnp.bfloat16)
-    weights = jax.nn.sigmoid(
-        jnp.stack(
-            [route_logits[:, 0] - route_logits[:, 1], route_logits[:, 1] - route_logits[:, 0]],
-            axis=1,
-        )
-    )
-    experts = lax.axis_size("sp") * w_gate.shape[0]
-    capacity = 4 * own_rows // experts
     slot_width = experts * capacity
     model = stream.shape[1]
     own_slots = slot_numbers(routes, experts, capacity)

time: 249 us -> 115 us (0.46)
  waiting for transfers between devices: 81 us -> 0 us
  matrix products: 44 us -> 0 us
  Pallas kernels: 85.4 us -> 101 us
  between operations: 13.5 us -> 0.05 us
  other arithmetic: 10.6 us -> 1.32 us
    reduce_scatter x1 -> x0, waiting for transfers between devices: 44 us -> none  [shards(): lax.psum_scatter(jnp.dot(hidden, w_down[0], preferred_element_type=jnp.fl...]
    dot_general x4 -> x0, matrix products: 44 us -> none  [the longest x1 25.8 us: shards(): jnp.dot(hidden, w_down[0], preferred_element_type=jnp.float32)]
    all_gather x2 -> x0, waiting for transfers between devices: 36.3 us -> none  [the longest x1 36.3 us: shards(): lax.all_gather(arrived.reshape(-1, model), 'tp', axis=0, tiled=True)]
    pallas_call x6 -> x2, Pallas kernels: 85.4 us -> 101 us  [the longest x1 70.3 us: moe(): pl.pallas_call(moe_kernel, out_shape=jax.ShapeDtypeStruct((tokens, model)...]
    unnamed x15 -> x23, local copies, waits for them, and re-layouts: 0.42 us -> 11.7 us
    another operation x4 -> x0, other arithmetic: 3.96 us -> none  [the longest x1 1.6 us: mixer(): reads = jnp.stack(diagonal(readout_matrix[0]) + diagonal(readout_matrix[1]))]
    reshape x6 -> x2, local copies, waits for them, and re-layouts: 4.24 us -> 0.86 us  [the longest x1 0.73 us: mixer_block(): log_step.reshape(-1, 1)]
    gather x2 -> x0, local copies, waits for them, and re-layouts: 3.14 us -> none  [shards(): jnp.take(returned_result, own_slots, axis=0).astype(jnp.float32)]
  transfers between devices with their start and end apart: 3 -> 0, of which waited for: 2 -> 0; matrix products, arithmetic and copies ran while one was open for 7% -> 0% of each run, Pallas kernels for 12% -> 0%
where the time goes in v2:
time: 115 us
  Pallas kernels  101 us (88%)
  local copies, waits for them, and re-layouts  12.6 us (11%)
  other arithmetic  1.32 us (1%)
    pallas_call x1, Pallas kernels, moe(): pl.pallas_call(moe_kernel, out_shape=jax.ShapeDtypeStruct((tokens, model)...  70.3 us
    pallas_call x1, Pallas kernels, mixer_block(): pl.pallas_call(mixer_kernel, out_shape=(jax.ShapeDtypeStruct((own_rows, m...  30.5 us
    unnamed x23, local copies, waits for them, and re-layouts  11.7 us

profile of v2, /device:TPU:8, one launch (start us, length us, event | category | flops | bytes accessed | tf_op | source)
XLA Modules:
  0.0 114.7 jit_solution(1197376938935656927)
XLA Ops:
  0.0 0.8 copy.18.shift
  0.8 0.7 copy.19.log_step
  1.5 1.0 copy.17
  2.6 0.1 reshape.16
  2.7 0.0 copy-start
  2.7 1.2 %copy-done = bf16[256,2048]{1,0:T(8,128)(2,1)S(1)} copy-done((bf16[256,2048]{1,0:T(8,128)(2,1)S(1)}, bf16[256,2048]{1,0:T(8,128)(2,1)}, u32[]{:S(2)}) %copy-start) | copy-done | bytes 1048600
  3.9 0.0 copy-start.3
  3.9 0.9 copy-done.3
  4.9 0.0 copy-start.4
  4.9 0.9 copy-done.4
  5.8 0.0 copy-start.5
  5.8 0.9 copy-done.5
  6.7 0.0 copy-start.6
  6.7 0.7 copy-done.6
  7.4 0.0 copy-start.7
  7.4 0.7 copy-done.7
  8.1 0.0 copy-start.8
  8.1 0.7 copy-done.8
  8.8 0.0 copy-start.9
  8.8 0.7 copy-done.9
  9.5 30.5 %mixer.1 = (bf16[64,2048]{1,0:T(8,128)(2,1)S(1)}, bf16[64,2048]{1,0:T(8,128)(2,1)S(1)}) custom-call(bf16[256,256]{1,0:T(8,128)(2,1)S(1)} %copy-done.5, f32[256,16]{1,0:T(8,128)S(1)} %copy.18.shift, f32[16,64]{1,0:T(8,128)S(1)} %copy-done.6, f32[16,64]{1,0:T(8,128)S(1)} %copy-done.7, f32[16,1]{1,0:T(8,128)S(1)} %copy.19.log_step, ...), custom_call_target="tpu_custom_call" | custom-call | tf_op jit(solution)/shard_map/mixer/pallas_call | solution.py:799
  40.0 0.0 copy-start.1
  40.0 0.7 copy-done.1
  40.7 0.0 copy-start.2
  40.7 0.7 copy-done.2
  41.4 0.8 slice_subtract_fusion.1
  42.2 0.6 fusion.3.weights
  42.8 70.3 %experts.1 = bf16[64,2048]{1,0:T(8,128)(2,1)} custom-call(bf16[64,2048]{1,0:T(8,128)(2,1)} %copy-done.2, bf16[64,2048]{1,0:T(8,128)(2,1)} %copy-done.1, s32[2,64]{1,0:T(2,128)} %bitcast.22, f32[2,64]{1,0:T(2,128)} %fusion.3.weights, bf16[2048,1792]{1,0:T(8,128)(2,1)} %bitcast.19, bf16[2048,1792]{1,0:T(8,128)(2,1)} %bitcast.20, bf16[1792,2048]{1,0:T(8,128)(2,1)} %bitcast.21), custom_call_target="tpu_custom_call" | custom-call | tf_op jit(solution)/shard_map/experts/pallas_call | solution.py:510
  113.1 1.7 %copy.21 = bf16[64,2048]{1,0:T(8,128)(2,1)} copy(bf16[64,2048]{1,0:T(8,128)(2,1)} %experts.1) | data formatting | bytes 524288
Async XLA Ops:
  2.7 1.2 %copy-start = (bf16[256,2048]{1,0:T(8,128)(2,1)S(1)}, bf16[256,2048]{1,0:T(8,128)(2,1)}, u32[]{:S(2)}) copy-start(bf16[256,2048]{1,0:T(8,128)(2,1)} %out_proj.1) | copy-start | bytes 3145732
  3.9 0.9 copy-start.3
  4.9 0.9 copy-start.4
  5.8 0.9 copy-start.5
  6.7 0.7 copy-start.6
  7.4 0.7 copy-start.7
  8.1 0.7 copy-start.8
  8.8 0.7 copy-start.9
  40.0 0.7 copy-start.1
  40.7 0.7 copy-start.2

commit v3 on v0

--- a/solution.py
+++ b/solution.py
@@ -272,6 +272,544 @@
     ).astype(jnp.bfloat16)
 
 
+def flip(index, bits):
+    bit = 1
+    while bit <= bits:
+        if bits & bit:
+            index = index + bit - 2 * bit * (index // bit % 2)
+        bit *= 2
+    return index
+
+
+def plan(experts):
+    if experts == 8:
+        order, sends = (0, 1, 4, 2, 5, 6, 7, 3), (1, 4, 2, 5, 6, 7, 3)
+        near, far = (0, 0, 0, 1, 6, 12, 15, 17), (0, 0, 5, 7, 12, 17, 20, 23)
+    else:
+        order, sends = tuple(range(experts)), tuple(range(1, experts))
+        near = tuple(max(0, 4 * place - 12) for place in range(experts))
+        far = tuple(max(0, 4 * place - 6) for place in range(experts))
+    events = {slot: [] for slot in range(4 * experts)}
+    for place in range(experts):
+        if place > 1:
+            events[near[place]].append(("pass_on", order[place]))
+        if place > 0:
+            events[far[place]].append(("pass_far", order[place]))
+    late = []
+    for place in range(experts):
+        for name, slot in (("cross", 4 * place + 5), ("give_back", 4 * place + 10)):
+            if slot < 4 * experts:
+                events[slot].append((name, order[place]))
+            else:
+                late.append((slot, name, order[place]))
+    return order, sends, events, [item[1:] for item in sorted(late)]
+
+
+def same(shape, row, column):
+    rows = lax.broadcasted_iota(jnp.int32, shape, 0)
+    columns = lax.broadcasted_iota(jnp.int32, shape, 1)
+    return row(rows) == column(columns)
+
+
+def chain(later, earlier):
+    b_real, b_imaginary, y_real, y_imaginary = later
+    a_real, a_imaginary, x_real, x_imaginary = earlier
+    return (
+        b_real * a_real - b_imaginary * a_imaginary,
+        b_real * a_imaginary + b_imaginary * a_real,
+        b_real * x_real - b_imaginary * x_imaginary + y_real,
+        b_real * x_imaginary + b_imaginary * x_real + y_imaginary,
+    )
+
+
+KINDS = ("sp", "y", "core", "far", "core_back", "y_back", "sp_back")
+PARTS = 2
+
+
+def layer_kernel(
+    values_in, shift_in, real_in, imaginary_in, log_in, map_in, readout_in, skip_in, proj_in,
+    stream_in, gain_in, routes_in, logits_in, w_gate, w_up, w_down, out,
+    values, shift, pole_real, pole_imaginary, log_step, input_map, readout, skip,
+    stream, gain, routes, logits,
+    scale, drive_real, drive_imaginary, parts, total, gathered, activated, acts, proj,
+    gate, up, down, outgoing, rows, hidden, kept, given, from_core, to_y, from_y, back, returned,
+    in_sem, own_sem, tot_send, tot_recv, act_send, act_recv, proj_send, proj_recv,
+    load_sem, send_sem, recv_sem,
+):
+    positions, width = scale.shape
+    groups, states = pole_real.shape
+    channels = values.shape[1]
+    inner = channels // groups
+    tokens, model = out.shape
+    experts, capacity = outgoing.shape[:2]
+    hidden_width = gate.shape[1]
+    tile, wide_tile = hidden_width // 2, model // 2
+    depth = channels // (2 * PARTS)
+    place, share = lax.axis_index("sp"), lax.axis_index("tp")
+    names = [flip(place, bits) for bits in range(experts)]
+    shares = [flip(share, kind) for kind in range(4)]
+    partner, across_y = shares[1], shares[2]
+    order, sends, events, late = plan(experts)
+    float_dot = functools.partial(
+        jnp.dot, precision=TOP_PRECISION, preferred_element_type=jnp.float32
+    )
+
+    barrier = pltpu.get_barrier_semaphore()
+    for bits in range(1, experts):
+        pl.semaphore_signal(barrier, inc=1, device_id={"sp": names[bits]}, device_id_type=MESH)
+    for kind in range(1, 4):
+        pl.semaphore_signal(barrier, inc=1, device_id={"tp": shares[kind]}, device_id_type=MESH)
+
+    inputs = (
+        (values_in, values), (shift_in, shift), (real_in, pole_real),
+        (imaginary_in, pole_imaginary), (log_in, log_step), (map_in, input_map),
+        (readout_in, readout), (skip_in, skip), (stream_in, stream), (gain_in, gain),
+        (routes_in, routes), (logits_in, logits),
+    )
+    fetches = [
+        pltpu.make_async_copy(source, target, in_sem.at[number])
+        for number, (source, target) in enumerate(inputs)
+    ]
+    for fetch in fetches:
+        fetch.start()
+    own_proj = pltpu.make_async_copy(proj_in, proj.at[0], own_sem)
+    own_proj.start()
+
+    def load(number, step):
+        source, target = ((w_gate, gate), (w_up, up), (w_down, down))[number]
+        length = wide_tile if number == 2 else tile
+        columns = pl.ds(pl.multiple_of(step * length, 128), length)
+        return pltpu.make_async_copy(
+            source.at[:, columns], target.at[:, columns], load_sem.at[number, step]
+        )
+
+    def remote_copy(source, target, send, receive, peer):
+        return pltpu.make_async_remote_copy(
+            src_ref=source, dst_ref=target, send_sem=send, recv_sem=receive,
+            device_id=peer, device_id_type=MESH,
+        )
+
+    half = place % 2
+
+    def weights(kind, side, part):
+        which = half if side == 0 else 1 - half
+        start = pl.multiple_of((which * PARTS + part) * depth, depth)
+        span = pl.ds(start, depth)
+        number = part if kind == 4 else side * PARTS + part
+        if kind == 4:
+            source, target, peer = proj.at[2, span], proj.at[2, span], {"sp": names[1]}
+        elif kind == 3:
+            source, target, peer = proj.at[2, span], proj.at[3, span], {"tp": partner}
+        else:
+            source, target = proj_in.at[span], proj.at[kind, span]
+            peer = {"tp": shares[kind]}
+        return remote_copy(
+            source, target, proj_send.at[kind, number], proj_recv.at[kind, number], peer
+        )
+
+    pl.semaphore_wait(barrier, experts + 2)
+    for part in range(PARTS):
+        weights(2, 0, part).start()
+    for side in range(2):
+        for part in range(PARTS):
+            weights(1, side, part).start()
+    for step in range(2):
+        load(0, step).start()
+        load(1, step).start()
+    for step in range(2):
+        load(2, step).start()
+    for fetch in fetches:
+        fetch.wait()
+
+    spread = same((states, width), lambda r: r, lambda c: c % states)
+    spread_low = spread.astype(jnp.bfloat16)
+    group = same((groups, width), lambda r: r, lambda c: c // states)
+    block = same((channels, width), lambda r: r // inner, lambda c: c // states)
+    column = jnp.sum(
+        jnp.where(same((groups, groups), lambda r: r, lambda c: c), log_step[...], 0.0),
+        axis=1, keepdims=True,
+    )
+    real, imaginary = pole_real[...], pole_imaginary[...]
+    step_size = jnp.exp(column)
+    magnitude = jnp.exp(real * step_size)
+    factor_real = magnitude * jnp.cos(imaginary * step_size)
+    factor_imaginary = magnitude * jnp.sin(imaginary * step_size)
+    denominator = real * real + imaginary * imaginary
+    ratio_real = ((factor_real - 1.0) * real + factor_imaginary * imaginary) / denominator
+    ratio_imaginary = (factor_imaginary * real - (factor_real - 1.0) * imaginary) / denominator
+    ratio_real, ratio_imaginary = (
+        jnp.broadcast_to(ratio[:, None, :], (groups, inner, states)).reshape(channels, states)
+        for ratio in (ratio_real, ratio_imaginary)
+    )
+    map_real = ratio_real * input_map[0] - ratio_imaginary * input_map[1]
+    map_imaginary = ratio_real * input_map[1] + ratio_imaginary * input_map[0]
+    laid = float_dot(
+        jnp.concatenate([factor_real, factor_imaginary], axis=0), spread.astype(jnp.float32)
+    )
+    factor_real, factor_imaginary = (
+        jnp.sum(
+            jnp.where(group, laid[n * groups : (n + 1) * groups], 0.0), axis=0, keepdims=True
+        )
+        for n in range(2)
+    )
+
+    segment = positions // LANES
+    permute = same((positions, positions), lambda r: r % LANES * segment + r // LANES, lambda c: c)
+    entries = jnp.dot(
+        permute.astype(jnp.bfloat16), values[...], preferred_element_type=jnp.float32
+    ).astype(jnp.bfloat16)
+    growth = lax.dot_general(
+        permute.astype(jnp.float32), jnp.exp(shift[...]), (((1,), (1,)), ((), ())),
+        precision=TOP_PRECISION, preferred_element_type=jnp.float32,
+    )
+    scale[...] = float_dot(growth, group.astype(jnp.float32))
+
+    def diagonal(value):
+        return [
+            jnp.where(
+                block, jnp.dot(piece, spread_low, preferred_element_type=jnp.float32), 0.0
+            ).astype(jnp.bfloat16)
+            for piece in split(value)
+        ]
+
+    for target, value in ((drive_real, map_real), (drive_imaginary, map_imaginary)):
+        high, low = diagonal(value)
+        target[...] = jnp.dot(entries, high, preferred_element_type=jnp.float32) + jnp.dot(
+            entries, low, preferred_element_type=jnp.float32
+        )
+
+    wide = (LANES, width)
+    wide_real = jnp.broadcast_to(factor_real, wide)
+    wide_imaginary = jnp.broadcast_to(factor_imaginary, wide)
+
+    def first_pass(position, carry):
+        at = pl.ds(pl.multiple_of(position * LANES, LANES), LANES)
+        grow = scale[at, :]
+        item = (
+            grow * wide_real, grow * wide_imaginary, drive_real[at, :], drive_imaginary[at, :]
+        )
+        return chain(item, carry)
+
+    empty = jnp.zeros(wide, jnp.float32)
+    ends = lax.fori_loop(
+        0, segment, first_pass, (jnp.ones(wide, jnp.float32), empty, empty, empty)
+    )
+    for number, end in enumerate(ends):
+        parts[number] = end
+    run = tuple(end[0:1] for end in ends)
+    for number in range(1, LANES):
+        run = chain(tuple(end[number : number + 1] for end in ends), run)
+    total[...] = jnp.concatenate(run + (jnp.zeros((LANES - 4, width), jnp.float32),), axis=0)
+    gathered[place] = total[...]
+
+    def totals(bits):
+        return remote_copy(
+            total, gathered.at[place], tot_send.at[bits], tot_recv.at[bits], {"sp": names[bits]}
+        )
+
+    for bits in range(1, experts):
+        totals(bits).start()
+    reads = diagonal(readout[0]) + diagonal(readout[1])
+
+    def share_out(part):
+        weights(2, 0, part).wait_recv()
+        weights(4, 0, part).start()
+        weights(3, 0, part).start()
+
+    share_out(0)
+    for bits in range(1, experts):
+        totals(bits).wait_recv()
+
+    def before(position, carry):
+        real, imaginary = carry
+        item = gathered[position]
+        a_real, a_imaginary = item[0:1], item[1:2]
+        keep = position < place
+        return (
+            jnp.where(keep, a_real * real - a_imaginary * imaginary + item[2:3], real),
+            jnp.where(keep, a_real * imaginary + a_imaginary * real + item[3:4], imaginary),
+        )
+
+    none = jnp.zeros((1, width), jnp.float32)
+    real, imaginary = lax.fori_loop(0, experts - 1, before, (none, none))
+    reals, imaginaries = [real], [imaginary]
+    for number in range(LANES - 1):
+        at = slice(number, number + 1)
+        a_real, a_imaginary = parts[0, at, :], parts[1, at, :]
+        real, imaginary = (
+            a_real * real - a_imaginary * imaginary + parts[2, at, :],
+            a_real * imaginary + a_imaginary * real + parts[3, at, :],
+        )
+        reals.append(real)
+        imaginaries.append(imaginary)
+
+    def second_pass(position, carry):
+        x_real, x_imaginary = carry
+        at = pl.ds(pl.multiple_of(position * LANES, LANES), LANES)
+        grow = scale[at, :]
+        b_real, b_imaginary = grow * wide_real, grow * wide_imaginary
+        new_real = b_real * x_real - b_imaginary * x_imaginary + drive_real[at, :]
+        new_imaginary = b_real * x_imaginary + b_imaginary * x_real + drive_imaginary[at, :]
+        drive_real[at, :] = new_real
+        drive_imaginary[at, :] = new_imaginary
+        return new_real, new_imaginary
+
+    lax.fori_loop(
+        0,
+        segment,
+        second_pass,
+        (jnp.concatenate(reals, axis=0), jnp.concatenate(imaginaries, axis=0)),
+    )
+    share_out(1)
+    high, low = split(drive_real[...])
+    response = across(high, reads[0]) + across(low, reads[0]) + across(high, reads[1])
+    high, low = split(drive_imaginary[...])
+    response -= across(high, reads[2]) + across(low, reads[2]) + across(high, reads[3])
+    response += skip[...] * entries.astype(jnp.float32)
+    restore = same((positions, positions), lambda r: r, lambda c: c % LANES * segment + c // LANES)
+    activated[...] = jnp.dot(
+        restore.astype(jnp.bfloat16),
+        jax.nn.gelu(response).astype(jnp.bfloat16),
+        preferred_element_type=jnp.float32,
+    ).astype(jnp.bfloat16)
+
+    def hand(kind):
+        start = pl.multiple_of(shares[kind] * tokens, tokens)
+        return remote_copy(
+            activated.at[pl.ds(start, tokens)], acts.at[kind], act_send.at[kind],
+            act_recv.at[kind], {"tp": shares[kind]},
+        )
+
+    for kind in range(1, 4):
+        hand(kind).start()
+    acts[0] = activated[pl.ds(pl.multiple_of(share * tokens, tokens), tokens), :]
+    own_proj.wait()
+    for part in range(PARTS):
+        weights(4, 1, part).wait_recv()
+        weights(3, 1, part).start()
+    projected = jnp.dot(acts[0], proj[0], preferred_element_type=jnp.float32)
+    for kind in range(1, 4):
+        hand(kind).wait_recv()
+        for side in range(2):
+            for part in range(PARTS):
+                if kind != 2:
+                    weights(kind, side, part).wait_recv()
+        projected += jnp.dot(acts[kind], proj[kind], preferred_element_type=jnp.float32)
+    mixed = (stream[...].astype(jnp.float32) + projected).astype(jnp.bfloat16).astype(jnp.float32)
+    normed = (
+        mixed * lax.rsqrt(jnp.mean(mixed * mixed, axis=-1, keepdims=True) + EPS) * gain[...]
+    ).astype(jnp.bfloat16)
+    out[...] = mixed
+
+    first, second = routes[0:1, :], routes[1:2, :]
+    gap = logits[0:1, :] - logits[1:2, :]
+    first_weight, second_weight = jax.nn.sigmoid(gap), jax.nn.sigmoid(-gap)
+    named = jnp.concatenate(
+        [((first == name) | (second == name)).astype(jnp.float32) for name in names], axis=0
+    )
+    earlier = (
+        lax.broadcasted_iota(jnp.int32, (tokens, tokens), 0)
+        < lax.broadcasted_iota(jnp.int32, (tokens, tokens), 1)
+    ).astype(jnp.float32)
+    rank = jnp.dot(named, earlier, preferred_element_type=jnp.float32).astype(jnp.int32)
+    scale = jnp.concatenate(
+        [
+            jnp.where(first == name, first_weight, 0.0)
+            + jnp.where(second == name, second_weight, 0.0)
+            for name in names
+        ],
+        axis=0,
+    )
+    slot = lax.broadcasted_iota(jnp.int32, (capacity, tokens), 0)
+    hits = [
+        jnp.where(slot == rank[e : e + 1, :], named[e : e + 1, :], 0.0) for e in range(experts)
+    ]
+    combine = jnp.concatenate([hit * scale[e : e + 1, :] for e, hit in enumerate(hits)], axis=0)
+    outgoing[...] = (
+        jnp.dot(
+            jnp.concatenate(hits, axis=0).astype(jnp.bfloat16),
+            normed,
+            preferred_element_type=jnp.float32,
+        )
+        .astype(jnp.bfloat16)
+        .reshape(outgoing.shape)
+    )
+    spot = (0, 2, 1, 3)
+
+    def at(bits, kind):
+        return rows.at[bits, pl.ds(spot[kind] * capacity, capacity)]
+
+    def remote(kind, bits):
+        source, target, peer = {
+            "sp": lambda: (outgoing.at[bits], at(bits, 0), {"sp": names[bits]}),
+            "y": lambda: (at(bits, 0), at(bits, 2), {"tp": across_y}),
+            "core": lambda: (at(bits, 0), at(bits, 1), {"tp": partner}),
+            "far": lambda: (at(bits, 2), at(bits, 3), {"tp": partner}),
+            "core_back": lambda: (given.at[bits], from_core.at[bits], {"tp": partner}),
+            "y_back": lambda: (to_y.at[bits], from_y.at[bits], {"tp": across_y}),
+            "sp_back": lambda: (back.at[bits], returned.at[bits], {"sp": names[bits]}),
+        }[kind]()
+        if bits == 0 and kind in ("y", "core"):
+            source = outgoing.at[0]
+        number = KINDS.index(kind)
+        return remote_copy(
+            source, target, send_sem.at[number, bits], recv_sem.at[number, bits], peer
+        )
+
+    def pass_on(bits):
+        if bits:
+            remote("sp", bits).wait_recv()
+        remote("y", bits).start()
+        remote("core", bits).start()
+
+    def pass_far(bits):
+        remote("y", bits).wait_recv()
+        remote("far", bits).start()
+
+    def cross(bits):
+        remote("core_back", bits).wait_recv()
+        to_y[bits] = (
+            kept[bits, capacity:, :] + from_core[bits, capacity:, :].astype(jnp.float32)
+        ).astype(jnp.bfloat16)
+        remote("y_back", bits).start()
+
+    def give_back(bits):
+        remote("y_back", bits).wait_recv()
+        total = (
+            kept[bits, :capacity, :]
+            + from_core[bits, :capacity, :].astype(jnp.float32)
+            + from_y[bits].astype(jnp.float32)
+        ).astype(jnp.bfloat16)
+        if bits:
+            back[bits] = total
+            remote("sp_back", bits).start()
+        else:
+            returned[0] = total
+
+    deeds = {"pass_on": pass_on, "pass_far": pass_far, "cross": cross, "give_back": give_back}
+
+    def act(step, slots):
+        for number, slot in enumerate(slots):
+            if events[slot]:
+                @pl.when(step == number)
+                def _():
+                    for name, bits in events[slot]:
+                        deeds[name](bits)
+
+    pass_on(0)
+    for bits in sends:
+        remote("sp", bits).start()
+    rows[0, 0:capacity, :] = outgoing[0]
+    pass_on(order[1])
+    pass_far(0)
+    for number, bits in enumerate(order):
+        remote("core", bits).wait_recv()
+        remote("far", bits).wait_recv()
+
+        def widen(step, carry):
+            columns = pl.ds(pl.multiple_of(step * tile, 128), tile)
+            if number == 0:
+                load(0, step).wait()
+                load(1, step).wait()
+            value = rows[bits]
+            opened = jnp.dot(value, gate[:, columns], preferred_element_type=jnp.float32)
+            raised = jnp.dot(value, up[:, columns], preferred_element_type=jnp.float32)
+            hidden[:, columns] = (jax.nn.silu(opened) * raised).astype(jnp.bfloat16)
+            act(step, (4 * number, 4 * number + 1))
+            return carry
+
+        lax.fori_loop(0, 2, widen, 0)
+
+        def narrow(step, carry):
+            columns = pl.ds(pl.multiple_of(step * wide_tile, 128), wide_tile)
+            if number == 0:
+                load(2, step).wait()
+            value = jnp.dot(hidden[...], down[:, columns], preferred_element_type=jnp.float32)
+            kept[bits, :, columns] = value[: 2 * capacity]
+            given[bits, :, columns] = value[2 * capacity :].astype(jnp.bfloat16)
+            act(step, (4 * number + 2, 4 * number + 3))
+            return carry
+
+        lax.fori_loop(0, 2, narrow, 0)
+        remote("core_back", bits).start()
+    for name, bits in late:
+        deeds[name](bits)
+    for bits in sends:
+        remote("sp_back", bits).wait_recv()
+    result = out[...]
+    every = returned[...].reshape(experts * capacity, model)
+    for piece in split(combine):
+        result += lax.dot_general(
+            piece, every, (((0,), (0,)), ((), ())), preferred_element_type=jnp.float32
+        )
+    out[...] = result
+    for bits in range(experts):
+        for kind in KINDS:
+            if bits or kind not in ("sp", "sp_back"):
+                remote(kind, bits).wait_send()
+    for bits in range(1, experts):
+        totals(bits).wait_send()
+    for kind in range(1, 4):
+        hand(kind).wait_send()
+    for side in range(2):
+        for part in range(PARTS):
+            weights(1, side, part).wait_send()
+            weights(3, side, part).wait_send()
+    for part in range(PARTS):
+        weights(2, 0, part).wait_send()
+        weights(4, 0, part).wait_send()
+
+
+def fits(shares, experts, capacity, w_gate):
+    if shares != 4 or w_gate.shape[0] != 1 or experts & (experts - 1) or experts < 2:
+        return False
+    return capacity % 16 == 0 and w_gate.shape[2] % 256 == 0 and w_gate.shape[1] % 256 == 0
+
+
+def layer(operands, number):
+    (values, shift, pole_real, pole_imaginary, log_step, input_map, readout, skip, out_proj,
+     stream, gain, routes, logits, w_gate, w_up, w_down) = operands
+    positions, channels = values.shape
+    groups, states = pole_real.shape
+    width = groups * states
+    experts = lax.axis_size("sp")
+    tokens, model = stream.shape
+    capacity = 4 * tokens // experts
+    hidden_width = w_gate.shape[1]
+    bf16, f32 = jnp.bfloat16, jnp.float32
+    dma = pltpu.SemaphoreType.DMA
+    inputs = (
+        values, shift, pole_real, pole_imaginary, log_step, input_map, readout, skip, stream,
+        gain, routes, logits,
+    )
+    arrays = [
+        ((positions, width), f32), ((positions, width), f32), ((positions, width), f32),
+        ((4, LANES, width), f32), ((LANES, width), f32), ((experts, LANES, width), f32),
+        ((positions, channels), bf16), ((4, tokens, channels), bf16), ((4, channels, model), bf16),
+        ((model, hidden_width), bf16), ((model, hidden_width), bf16), ((hidden_width, model), bf16),
+        ((experts, capacity, model), bf16), ((experts, 4 * capacity, model), bf16),
+        ((4 * capacity, hidden_width), bf16), ((experts, 2 * capacity, model), f32),
+        ((experts, 2 * capacity, model), bf16), ((experts, 2 * capacity, model), bf16),
+    ] + [((experts, capacity, model), bf16)] * 4
+    return pl.pallas_call(
+        layer_kernel,
+        out_shape=jax.ShapeDtypeStruct((tokens, model), f32),
+        in_specs=[pl.BlockSpec(memory_space=pl.ANY)] * len(operands),
+        out_specs=pl.BlockSpec(memory_space=pltpu.VMEM),
+        scratch_shapes=[pltpu.VMEM(value.shape, value.dtype) for value in inputs]
+        + [pltpu.VMEM(shape, kind) for shape, kind in arrays]
+        + [
+            dma((len(inputs),)), dma, dma((experts,)), dma((experts,)), dma((4,)), dma((4,)),
+            dma((5, 2 * PARTS)), dma((5, 2 * PARTS)), dma((3, 2)),
+            dma((len(KINDS), experts)), dma((len(KINDS), experts)),
+        ],
+        compiler_params=pltpu.CompilerParams(
+            collective_id=number, has_side_effects=True, vmem_limit_bytes=63 * 2**20
+        ),
+        name="layer",
+    )(*operands)
+
+
 def shards(
     mixer_input,
     decay_shift,
@@ -290,9 +828,20 @@
     w_up,
     w_down,
 ):
-    factors = discretize(pole_real, pole_imaginary, log_step, input_map)
     shares = lax.axis_size("tp")
     own_rows = stream.shape[0]
+    experts = lax.axis_size("sp") * w_gate.shape[0]
+    capacity = 4 * own_rows // experts
+    if fits(shares, experts, capacity, w_gate):
+        channels, (groups, states) = mixer_input.shape[1], pole_real.shape
+        operands = (
+            mixer_input, decay_shift.T, pole_real, pole_imaginary, log_step.reshape(1, -1),
+            jnp.swapaxes(input_map, 2, 3).reshape(2, channels, states),
+            readout_matrix.reshape(2, channels, states), skip.reshape(1, -1), out_proj, stream,
+            norm_gain.reshape(1, -1), routes.T, route_logits.T, w_gate[0], w_up[0], w_down[0],
+        )
+        return layer(operands, 4).astype(jnp.bfloat16)
+    factors = discretize(pole_real, pole_imaginary, log_step, input_map)
     activated = mixer(mixer_input, decay_shift, factors, readout_matrix, skip)
     whole_proj = lax.all_gather(out_proj, "tp", axis=0, tiled=True)
     received = exchange(activated.reshape(shares, own_rows, -1), "tp", 1)
@@ -311,8 +860,6 @@
             axis=1,
         )
     )
-    experts = lax.axis_size("sp") * w_gate.shape[0]
-    capacity = 4 * own_rows // experts
     slot_width = experts * capacity
     model = stream.shape[1]
     own_slots = slot_numbers(routes, experts, capacity)

time: 249 us -> 95.9 us (0.39)
  waiting for transfers between devices: 81 us -> 0 us
  matrix products: 44 us -> 0 us
  between operations: 13.5 us -> 0.01 us
  local copies, waits for them, and re-layouts: 12.6 us -> 0 us
  other arithmetic: 10.6 us -> 1.77 us
  Pallas kernels: 85.4 us -> 93.8 us
    reduce_scatter x1 -> x0, waiting for transfers between devices: 44 us -> none  [shards(): lax.psum_scatter(jnp.dot(hidden, w_down[0], preferred_element_type=jnp.fl...]
    dot_general x4 -> x0, matrix products: 44 us -> none  [the longest x1 25.8 us: shards(): jnp.dot(hidden, w_down[0], preferred_element_type=jnp.float32)]
    all_gather x2 -> x0, waiting for transfers between devices: 36.3 us -> none  [the longest x1 36.3 us: shards(): lax.all_gather(arrived.reshape(-1, model), 'tp', axis=0, tiled=True)]
    pallas_call x6 -> x1, Pallas kernels: 85.4 us -> 93.8 us  [layer(): pl.pallas_call(layer_kernel, out_shape=jax.ShapeDtypeStruct((tokens, mode...]
    reshape x6 -> x0, local copies, waits for them, and re-layouts: 4.24 us -> none  [the longest x1 1.6 us: mixer(): return jnp.swapaxes(activated.reshape(rows // LANES, LANES, channels), 0, 1)]
    another operation x4 -> x0, other arithmetic: 3.96 us -> none  [the longest x1 1.6 us: mixer(): reads = jnp.stack(diagonal(readout_matrix[0]) + diagonal(readout_matrix[1]))]
    gather x2 -> x0, local copies, waits for them, and re-layouts: 3.14 us -> none  [shards(): jnp.take(returned_result, own_slots, axis=0).astype(jnp.float32)]
    reduce_sum x3 -> x0, other arithmetic: 2.59 us -> none  [the longest x1 2.33 us: shards(): combined = mixed_wide + jnp.sum(picked * weights[:, :, None], axis=1)]
  transfers between devices with their start and end apart: 3 -> 0, of which waited for: 2 -> 0; matrix products, arithmetic and copies ran while one was open for 7% -> 0% of each run, Pallas kernels for 12% -> 0%
where the time goes in v3:
time: 95.9 us; the launch traced here: 95.6 us
  Pallas kernels  93.8 us (98%)
  other arithmetic  1.77 us (2%)
    pallas_call x1, Pallas kernels, layer(): pl.pallas_call(layer_kernel, out_shape=jax.ShapeDtypeStruct((tokens, mode...  93.8 us

profile of v3, /device:TPU:8, one launch (start us, length us, event | category | flops | bytes accessed | tf_op | source)
XLA Modules:
  0.0 95.6 jit_solution(7593781805334747278)
XLA Ops:
  0.0 93.8 %layer.1 = f32[64,2048]{1,0:T(8,128)} custom-call(bf16[256,256]{1,0:T(8,128)(2,1)} %values_in.1, f32[16,256]{1,0:T(8,128)} %bitcast.18, f32[16,64]{1,0:T(8,128)} %real_in.1, f32[16,64]{1,0:T(8,128)} %imaginary_in.1, f32[1,16]{1,0:T(1,128)} %bitcast.23, f32[2,256,64]{2,1,0:T(8,128)} %bitcast.16, f32[2,256,64]{2,1,0:T(8,128)} %bitcast.17, f32[1,256]{1,0:T(1,128)} %bitcast.20, ...), custom_call_target="tpu_custom_call" | custom-call | tf_op jit(solution)/shard_map/layer/pallas_call | solution.py:794
  93.8 1.8 %convert_element_type.3 = bf16[64,2048]{1,0:T(8,128)(2,1)} convert(f32[64,2048]{1,0:T(8,128)} %layer.1) | non-fusion elementwise | flops 131072 | bytes 786432 | tf_op jit(solution)/shard_map/convert_element_type | solution.py:843

commit v4 on v3

--- a/solution.py
+++ b/solution.py
@@ -283,8 +283,8 @@
 
 def plan(experts):
     if experts == 8:
-        order, sends = (0, 1, 4, 2, 5, 6, 7, 3), (1, 4, 2, 5, 6, 7, 3)
-        near, far = (0, 0, 0, 1, 6, 12, 15, 17), (0, 0, 5, 7, 12, 17, 20, 23)
+        order, sends = (0, 1, 4, 2, 5, 3, 6, 7), (4, 1, 2, 5, 3, 6, 7)
+        near, far = (0, 0, 0, 1, 6, 9, 13, 17), (0, 0, 5, 7, 12, 14, 19, 22)
     else:
         order, sends = tuple(range(experts)), tuple(range(1, experts))
         near = tuple(max(0, 4 * place - 12) for place in range(experts))
@@ -297,7 +297,7 @@
             events[far[place]].append(("pass_far", order[place]))
     late = []
     for place in range(experts):
-        for name, slot in (("cross", 4 * place + 5), ("give_back", 4 * place + 10)):
+        for name, slot in (("cross", 4 * place + 5), ("give_back", 4 * place + 12)):
             if slot < 4 * experts:
                 events[slot].append((name, order[place]))
             else:
@@ -324,6 +324,7 @@
 
 KINDS = ("sp", "y", "core", "far", "core_back", "y_back", "sp_back")
 PARTS = 2
+PIECES = ((0, 0), (0, 1), (1, 0), (1, 1), (2, 0))
 
 
 def layer_kernel(
@@ -344,7 +345,6 @@
     experts, capacity = outgoing.shape[:2]
     hidden_width = gate.shape[1]
     tile, wide_tile = hidden_width // 2, model // 2
-    depth = channels // (2 * PARTS)
     place, share = lax.axis_index("sp"), lax.axis_index("tp")
     names = [flip(place, bits) for bits in range(experts)]
     shares = [flip(share, kind) for kind in range(4)]
@@ -390,11 +390,17 @@
         )
 
     half = place % 2
+    unit = channels // 16
 
     def weights(kind, side, part):
-        which = half if side == 0 else 1 - half
-        start = pl.multiple_of((which * PARTS + part) * depth, depth)
-        span = pl.ds(start, depth)
+        if kind == 1:
+            span = pl.ds(0, channels)
+        elif side == 2:
+            span = pl.ds(6 * unit, 4 * unit)
+        else:
+            which = half if side == 0 else 1 - half
+            start = pl.multiple_of(which * 10 * unit + part * 3 * unit, unit)
+            span = pl.ds(start, 3 * unit)
         number = part if kind == 4 else side * PARTS + part
         if kind == 4:
             source, target, peer = proj.at[2, span], proj.at[2, span], {"sp": names[1]}
@@ -408,11 +414,9 @@
         )
 
     pl.semaphore_wait(barrier, experts + 2)
-    for part in range(PARTS):
-        weights(2, 0, part).start()
-    for side in range(2):
-        for part in range(PARTS):
-            weights(1, side, part).start()
+    for side, part in ((0, 0), (0, 1), (2, 0)):
+        weights(2, side, part).start()
+    weights(1, 0, 0).start()
     for step in range(2):
         load(0, step).start()
         load(1, step).start()
@@ -584,16 +588,19 @@
         hand(kind).start()
     acts[0] = activated[pl.ds(pl.multiple_of(share * tokens, tokens), tokens), :]
     own_proj.wait()
+    weights(2, 2, 0).wait_recv()
+    weights(3, 2, 0).start()
     for part in range(PARTS):
         weights(4, 1, part).wait_recv()
         weights(3, 1, part).start()
     projected = jnp.dot(acts[0], proj[0], preferred_element_type=jnp.float32)
     for kind in range(1, 4):
         hand(kind).wait_recv()
-        for side in range(2):
-            for part in range(PARTS):
-                if kind != 2:
-                    weights(kind, side, part).wait_recv()
+        if kind == 1:
+            weights(1, 0, 0).wait_recv()
+        if kind == 3:
+            for side, part in PIECES:
+                weights(3, side, part).wait_recv()
         projected += jnp.dot(acts[kind], proj[kind], preferred_element_type=jnp.float32)
     mixed = (stream[...].astype(jnp.float32) + projected).astype(jnp.bfloat16).astype(jnp.float32)
     normed = (
@@ -751,13 +758,13 @@
         totals(bits).wait_send()
     for kind in range(1, 4):
         hand(kind).wait_send()
-    for side in range(2):
-        for part in range(PARTS):
-            weights(1, side, part).wait_send()
-            weights(3, side, part).wait_send()
-    for part in range(PARTS):
-        weights(2, 0, part).wait_send()
-        weights(4, 0, part).wait_send()
+    weights(1, 0, 0).wait_send()
+    for side, part in PIECES:
+        weights(3, side, part).wait_send()
+        if side != 1:
+            weights(2, side, part).wait_send()
+        if side == 0:
+            weights(4, side, part).wait_send()
 
 
 def fits(shares, experts, capacity, w_gate):
@@ -800,7 +807,7 @@
         + [pltpu.VMEM(shape, kind) for shape, kind in arrays]
         + [
             dma((len(inputs),)), dma, dma((experts,)), dma((experts,)), dma((4,)), dma((4,)),
-            dma((5, 2 * PARTS)), dma((5, 2 * PARTS)), dma((3, 2)),
+            dma((5, len(PIECES))), dma((5, len(PIECES))), dma((3, 2)),
             dma((len(KINDS), experts)), dma((len(KINDS), experts)),
         ],
         compiler_params=pltpu.CompilerParams(

time: 95.9 us -> 90.3 us (0.942)
  Pallas kernels: 93.8 us -> 88.4 us
    pallas_call x1, Pallas kernels: 93.8 us -> 88.4 us  [layer(): pl.pallas_call(layer_kernel, out_shape=jax.ShapeDtypeStruct((tokens, mode...]
where the time goes in v4:
time: 90.3 us; the launch traced here: 90.2 us
  Pallas kernels  88.4 us (98%)
  other arithmetic  1.77 us (2%)
    pallas_call x1, Pallas kernels, layer(): pl.pallas_call(layer_kernel, out_shape=jax.ShapeDtypeStruct((tokens, mode...  88.4 us

profile of v4, /device:TPU:8, one launch (start us, length us, event | category | flops | bytes accessed | tf_op | source)
XLA Modules:
  0.0 90.2 jit_solution(861239540093141819)
XLA Ops:
  0.0 88.4 %layer.1 = f32[64,2048]{1,0:T(8,128)} custom-call(bf16[256,256]{1,0:T(8,128)(2,1)} %values_in.1, f32[16,256]{1,0:T(8,128)} %bitcast.18, f32[16,64]{1,0:T(8,128)} %real_in.1, f32[16,64]{1,0:T(8,128)} %imaginary_in.1, f32[1,16]{1,0:T(1,128)} %bitcast.23, f32[2,256,64]{2,1,0:T(8,128)} %bitcast.16, f32[2,256,64]{2,1,0:T(8,128)} %bitcast.17, f32[1,256]{1,0:T(1,128)} %bitcast.20, ...), custom_call_target="tpu_custom_call" | custom-call | tf_op jit(solution)/shard_map/layer/pallas_call | solution.py:801
  88.4 1.8 %convert_element_type.3 = bf16[64,2048]{1,0:T(8,128)(2,1)} convert(f32[64,2048]{1,0:T(8,128)} %layer.1) | non-fusion elementwise | flops 131072 | bytes 786432 | tf_op jit(solution)/shard_map/convert_element_type | solution.py:850
